TPU v7x, 512 devices: a whole 4x4x16 slice. The times are simulated.
512 devices in a mesh: sp: 64 (over z, y), tp: 8 (over x, core).
Axes of the slice: x: 4, y: 4, z: 16, core: 2. Of those that a mesh axis runs over, the one named last changes fastest.
Arguments:
- residual: bfloat16 [24576, 2048], P('sp'), may hold values from -6 to 6
- queries: bfloat16 [24576, 2048], P('sp', 'tp'), may hold values from -48 to 48
- keys: bfloat16 [24576, 2048], P('sp', 'tp'), may hold values from -48 to 48
- values: bfloat16 [24576, 2048], P('sp', 'tp'), may hold values from -6 to 6
- gate_cache: float32 [24576, 32], P('sp', 'tp'), may hold values from -6152 to 0, as said below
- doc_ids: int32 [24576], P('sp'), may hold values from 0 to 31, never falling along the last dimension, each value on 1 to 1536 neighbouring positions
- out_weight: bfloat16 [2048, 2048], P('tp'), may hold values from -1 to 1
- mix_gain: float32 [2048], replicated, may hold values from 0.1 to 1.9
- gate_weight: bfloat16 [2048, 5120], P('sp', 'tp'), may hold values from -0.125 to 0.125
- up_weight: bfloat16 [2048, 5120], P('sp', 'tp'), may hold values from -0.125 to 0.125
- down_weight: bfloat16 [5120, 2048], P('tp', 'sp'), may hold values from -0.15625 to 0.15625
Outputs:
- layer_out: bfloat16 [24576, 2048], P(('sp', 'tp'))
Inputs may be any that keep to these rules, and one draw needn't show every extreme that they name: `doc_ids`: positions of one document are consecutive; each document has 1 to 1536 positions, and one has exactly that many. `gate_cache`: no column rises from one position to the next.
All inputs are finite; a program needn't handle non-finite values.
Results may differ from a plain program's by a relative error of at most 0.018.
Values may be sent and summed in bfloat16 or wider, within the bound.
A program may use at most 64 MiB of HBM per device.

v0:
```python
import jax
import jax.numpy as jnp
from jax import lax
from jax.sharding import Mesh
from jax.sharding import PartitionSpec as P

REACH = 4
SP = ("sp_0", "sp_1")
SP_TP = ("sp_0", "sp_1", "tp")


EPSILON = 1e-06
NEGATIVE = -1e30


def from_behind(value, axis, steps):
    count = lax.axis_size(axis)
    first, last = (max(0, -steps), min(count, count - steps))
    return lax.ppermute(value, axis, [(source, source + steps) for source in range(first, last)])


def in_blocks(shard, dim, size):
    before, after = (shard.shape[:dim], shard.shape[dim + 1 :])
    return jnp.moveaxis(shard.reshape(*before, size, -1, *after), dim, 0)


def sent_and_summed(shard, axis, dim):
    pieces = in_blocks(shard, dim, lax.axis_size(axis))
    arrived = lax.all_to_all(pieces, axis, split_axis=0, concat_axis=0, tiled=True)
    return arrived.astype(jnp.float32).sum(axis=0)


def joined_along(pieces, dim):
    shape = list(pieces.shape[1:])
    shape[dim] *= pieces.shape[0]
    return jnp.moveaxis(pieces, 0, dim).reshape(shape)


def copy_for_each(shard, axis):
    size = lax.axis_size(axis)
    return lax.all_to_all(
        jnp.broadcast_to(shard[None], (size, *shard.shape)), axis, 0, 0, tiled=True
    )


def gathered_copies(shard, axis, dim):
    return joined_along(copy_for_each(shard, axis), dim)


def in_one_piece(arrays, axis, dim, along):
    both = jnp.concatenate(arrays, axis=along)
    out, at, done = (lax.all_gather(both, axis, axis=dim, tiled=True), 0, [])
    for a in arrays:
        done.append(lax.slice_in_dim(out, at, at + a.shape[along], axis=along))
        at += a.shape[along]
    return tuple(done)


def whole_of(shard, axes, dim):
    for axis in reversed(axes):
        shard = lax.all_gather(shard, axis, axis=dim, tiled=True)
    return shard


def normalize(middle, gain):
    widened = middle.astype(jnp.float32)
    factor = lax.rsqrt(jnp.mean(widened * widened, axis=-1, keepdims=True) + EPSILON)
    return (widened * factor * gain).astype(jnp.bfloat16)


def local(
    residual,
    queries,
    keys,
    values,
    gate_cache,
    doc_ids,
    out_weight,
    mix_gain,
    gate_weight,
    up_weight,
    down_weight,
):
    tok_rows = queries.shape[0]
    heads_here = gate_cache.shape[1]
    head_size = queries.shape[1] // heads_here
    sp_index = lax.axis_index(SP)
    key_parts = [keys]
    value_parts = [values]
    cache_parts = [gate_cache]
    doc_parts = [doc_ids]
    for distance in range(1, REACH + 1):
        moved_keys, moved_values = from_behind((keys, values), SP, distance)
        moved_cache, moved_docs = from_behind((gate_cache, doc_ids), SP, distance)
        key_parts.append(moved_keys)
        value_parts.append(moved_values)
        cache_parts.append(moved_cache)
        doc_parts.append(moved_docs)
    all_keys = jnp.concatenate(key_parts[::-1], axis=0)
    all_values = jnp.concatenate(value_parts[::-1], axis=0)
    all_cache = jnp.concatenate(cache_parts[::-1], axis=0)
    all_docs = jnp.concatenate(doc_parts[::-1], axis=0)
    key_count = all_keys.shape[0]
    query_pos = sp_index * tok_rows + jnp.arange(tok_rows, dtype=jnp.int32)
    key_pos = (sp_index - REACH) * tok_rows + jnp.arange(key_count, dtype=jnp.int32)
    visible = (
        (key_pos[None, :] <= query_pos[:, None])
        & (key_pos[None, :] >= 0)
        & (all_docs[None, :] == doc_ids[:, None])
    )
    query_heads = queries.reshape(tok_rows, heads_here, head_size)
    key_heads = all_keys.reshape(key_count, heads_here, head_size)
    value_heads = all_values.reshape(key_count, heads_here, head_size)
    score_scale = head_size ** (-0.5)
    scores = (
        jnp.einsum("qhd,khd->hqk", query_heads, key_heads, preferred_element_type=jnp.float32)
        * score_scale
    )
    scores = scores + gate_cache.T[:, :, None] - all_cache.T[:, None, :]
    scores = jnp.where(visible[None], scores, NEGATIVE)
    row_max = jnp.max(scores, axis=-1, keepdims=True)
    exp_scores = jnp.exp(scores - row_max)
    weights = (exp_scores / jnp.sum(exp_scores, axis=-1, keepdims=True)).astype(jnp.bfloat16)
    attended = jnp.einsum("hqk,khd->qhd", weights, value_heads, preferred_element_type=jnp.float32)
    attended = attended.astype(jnp.bfloat16).reshape(tok_rows, heads_here * head_size)
    row_share = tok_rows // lax.axis_size("tp")
    tp_index = lax.axis_index("tp")
    attn_sum = sent_and_summed(
        jnp.dot(attended, out_weight, preferred_element_type=jnp.float32).astype(jnp.bfloat16),
        "tp",
        0,
    )
    own_rows = lax.dynamic_slice_in_dim(residual, tp_index * row_share, row_share, 0)
    middle = (own_rows.astype(jnp.float32) + attn_sum).astype(jnp.bfloat16)
    mixer_in = gathered_copies(normalize(middle, mix_gain), "tp", 0)
    held_gate, held_up = in_one_piece((gate_weight, up_weight), SP, 0, 1)
    gate_proj = jnp.dot(mixer_in, held_gate, preferred_element_type=jnp.float32)
    up_proj = jnp.dot(mixer_in, held_up, preferred_element_type=jnp.float32)
    hidden = (jax.nn.silu(gate_proj) * up_proj).astype(jnp.bfloat16)
    partials = jnp.dot(hidden, whole_of(down_weight, SP, 1), preferred_element_type=jnp.float32)
    down_sum = sent_and_summed(partials.astype(jnp.bfloat16), "tp", 0)
    return (middle.astype(jnp.float32) + down_sum).astype(jnp.bfloat16)


def solution(mesh):
    finer = Mesh(mesh.devices.reshape(16, 4, mesh.shape["tp"]), ("sp_0", "sp_1", "tp"))
    return jax.shard_map(
        local,
        mesh=finer,
        in_specs=(
            P(SP, None),
            P(SP, "tp"),
            P(SP, "tp"),
            P(SP, "tp"),
            P(SP, "tp"),
            P(SP),
            P("tp", None),
            P(),
            P(SP, "tp"),
            P(SP, "tp"),
            P("tp", SP),
        ),
        out_specs=P(SP_TP, None),
        check_vma=False,
    )
```

profile of v0, /device:TPU:1, one launch (start us, length us, event | category | flops | bytes accessed | tf_op | source)
XLA Modules:
  0.0 275.9 jit_solution(5888889209596359937)
XLA Ops:
  6.5 1.5 pad_maximum_fusion
  8.2 4.4 %collective-permute-start.4 = (s32[384]{0:T(512)}, s32[384]{0:T(512)S(1)}, u32[]{:S(2)}, u32[]{:S(2)}) collective-permute-start(s32[384]{0:T(512)} %param.16), channel_id=1, source_target_pairs={{0,32},{8,40},{16,48},{24,56},{32,64},{40,72},{48,80},{56,88},{64,... | collective-permute-start | bytes 4616 | tf_op jit(solution)/shard_map/ppermute | solution.py:19
  12.5 4.6 %collective-permute-start.5 = (s32[384]{0:T(512)}, s32[384]{0:T(512)S(1)}, u32[]{:S(2)}, u32[]{:S(2)}) collective-permute-start(s32[384]{0:T(512)} %param.16), channel_id=1, source_target_pairs={{0,24},{8,32},{16,40},{24,48},{32,56},{40,64},{48,72},{56,80},{64,... | collective-permute-start | bytes 4616 | tf_op jit(solution)/shard_map/ppermute | solution.py:19
  17.2 3.6 %collective-permute-start.6 = (s32[384]{0:T(512)}, s32[384]{0:T(512)S(1)}, u32[]{:S(2)}, u32[]{:S(2)}) collective-permute-start(s32[384]{0:T(512)} %param.16), channel_id=1, source_target_pairs={{0,16},{8,24},{16,32},{24,40},{32,48},{40,56},{48,64},{56,72},{64,... | collective-permute-start | bytes 4616 | tf_op jit(solution)/shard_map/ppermute | solution.py:19
  20.8 2.6 collective-permute-start.7
  23.4 3.6 %collective-permute-start.8 = (bf16[384,256]{1,0:T(8,128)(2,1)}, bf16[384,256]{1,0:T(8,128)(2,1)S(1)}, u32[]{:S(2)}, u32[]{:S(2)}) collective-permute-start(bf16[384,256]{1,0:T(8,128)(2,1)} %param.13), channel_id=1, source_target_pairs={{0,32},{8,40},{16,48},{24,56},{32,64},{40,72},{48,80},{56,88},{64,... | collective-permute-start | bytes 589832 | tf_op jit(solution)/shard_map/ppermute | solution.py:19
  27.0 13.7 %all_gather.10 = bf16[640,128]{0,1:T(8,128)(2,1)} all-gather(bf16[640,32]{0,1:T(8,128)(2,1)} %param.21), channel_id=1, replica_groups=mesh['sp_0'=16,'sp_1'=4,'tp'=8] {'sp_1'}, dimensions={1}, use_global_device_ids=true | all-gather | bytes 204800 | tf_op jit(solution)/shard_map/all_gather | solution.py:61
  40.8 1.1 copy.18
  41.9 3.6 %collective-permute-start.9 = (bf16[384,256]{1,0:T(8,128)(2,1)}, bf16[384,256]{1,0:T(8,128)(2,1)S(1)}, u32[]{:S(2)}, u32[]{:S(2)}) collective-permute-start(bf16[384,256]{1,0:T(8,128)(2,1)} %param.13), channel_id=1, source_target_pairs={{0,24},{8,32},{16,40},{24,48},{32,56},{40,64},{48,72},{56,80},{64,... | collective-permute-start | bytes 589832 | tf_op jit(solution)/shard_map/ppermute | solution.py:19
  45.5 3.9 %collective-permute-start.10 = (bf16[384,256]{1,0:T(8,128)(2,1)}, bf16[384,256]{1,0:T(8,128)(2,1)S(1)}, u32[]{:S(2)}, u32[]{:S(2)}) collective-permute-start(bf16[384,256]{1,0:T(8,128)(2,1)} %param.13), channel_id=1, source_target_pairs={{0,16},{8,24},{16,32},{24,40},{32,48},{40,56},{48,64},{56,72},{64,... | collective-permute-start | bytes 589832 | tf_op jit(solution)/shard_map/ppermute | solution.py:19
  49.4 1.8 collective-permute-start.11
  51.2 3.6 %collective-permute-start.12 = (f32[384,4]{0,1:T(4,128)}, f32[384,4]{0,1:T(4,128)S(1)}, u32[]{:S(2)}, u32[]{:S(2)}) collective-permute-start(f32[384,4]{0,1:T(4,128)} %param.15), channel_id=1, source_target_pairs={{0,32},{8,40},{16,48},{24,56},{32,64},{40,72},{48,80},{56,88},{64,... | collective-permute-start | bytes 18440 | tf_op jit(solution)/shard_map/ppermute | solution.py:19
  55.6 3.3 %compare_and_fusion = pred[384,1920]{0,1:T(8,128)(4,1)} fusion(s32[384]{0:T(512)} %param.16, s32[384]{0:T(512)S(1)} %iota_add_fusion.1, s32[1920]{0:T(1024)S(1)} %constant_dynamic-update-slice_fusion.16, s32[1920]{0:T(1024)S(1)} %iota_add_fusion, pred[1920]{0:T(1024)(128)(4,1)S(1)} %broadcast_compare_fusion), kind=kLoop, calls=%fused_computation.13 | loop fusion | flops 2949120 | bytes 757632 | tf_op jit(solution)/shard_map/and | solution.py:107
  58.8 5.5 %collective-permute-start.13 = (f32[384,4]{0,1:T(4,128)}, f32[384,4]{0,1:T(4,128)S(1)}, u32[]{:S(2)}, u32[]{:S(2)}) collective-permute-start(f32[384,4]{0,1:T(4,128)} %param.15), channel_id=1, source_target_pairs={{0,24},{8,32},{16,40},{24,48},{32,56},{40,64},{48,72},{56,80},{64,... | collective-permute-start | bytes 18440 | tf_op jit(solution)/shard_map/ppermute | solution.py:19
  65.3 3.1 %collective-permute-start.14 = (f32[384,4]{0,1:T(4,128)}, f32[384,4]{0,1:T(4,128)S(1)}, u32[]{:S(2)}, u32[]{:S(2)}) collective-permute-start(f32[384,4]{0,1:T(4,128)} %param.15), channel_id=1, source_target_pairs={{0,16},{8,24},{16,32},{24,40},{32,48},{40,56},{48,64},{56,72},{64,... | collective-permute-start | bytes 18440 | tf_op jit(solution)/shard_map/ppermute | solution.py:19
  69.4 4.7 %collective-permute-start.15 = (f32[384,4]{0,1:T(4,128)}, f32[384,4]{0,1:T(4,128)S(1)}, u32[]{:S(2)}, u32[]{:S(2)}) collective-permute-start(f32[384,4]{0,1:T(4,128)} %param.15), channel_id=1, source_target_pairs={{0,8},{8,16},{16,24},{24,32},{32,40},{40,48},{48,56},{56,64},{64,7... | collective-permute-start | bytes 18440 | tf_op jit(solution)/shard_map/ppermute | solution.py:19
  75.1 10.1 %collective-permute-start = (bf16[384,256]{1,0:T(8,128)(2,1)}, bf16[384,256]{1,0:T(8,128)(2,1)}, u32[]{:S(2)}, u32[]{:S(2)}) collective-permute-start(bf16[384,256]{1,0:T(8,128)(2,1)} %param.14), channel_id=1, source_target_pairs={{0,32},{8,40},{16,48},{24,56},{32,64},{40,72},{48,80},{56,88},{64,... | collective-permute-start | bytes 589832 | tf_op jit(solution)/shard_map/ppermute | solution.py:19
  85.9 2.7 collective-permute-start.1
  88.7 3.6 %collective-permute-start.2 = (bf16[384,256]{1,0:T(8,128)(2,1)}, bf16[384,256]{1,0:T(8,128)(2,1)}, u32[]{:S(2)}, u32[]{:S(2)}) collective-permute-start(bf16[384,256]{1,0:T(8,128)(2,1)} %param.14), channel_id=1, source_target_pairs={{0,16},{8,24},{16,32},{24,40},{32,48},{40,56},{48,64},{56,72},{64,... | collective-permute-start | bytes 589832 | tf_op jit(solution)/shard_map/ppermute | solution.py:19
  92.3 2.0 collective-permute-start.3
  95.1 7.0 %fusion.36 = f32[4,384]{1,0:T(4,128)S(1)} fusion(f32[4,1920]{1,0:T(4,128)S(1)} %bitcast.44, f32[4,384]{1,0:T(4,128)S(1)} %bitcast.42, pred[384,1920]{0,1:T(8,128)(4,1)} %compare_and_fusion, bf16[1920,4,64]{0,2,1:T(8,128)(2,1)S(1)} %bitcast.36, bf16[384,4,64]{0,2,1:T(8,128)(2,1)S(1)} %bitcast.39), kind=kOutput, calls=%fused_computation.64 | convolution fusion | flops 395184000 | bytes 1959936 | tf_op jit(solution)/shard_map/sub | solution.py:122
  106.0 1.4 copy.16
  107.4 7.7 %fusion.20 = bf16[4,64,384]{2,1,0:T(8,128)(2,1)S(1)} fusion(bf16[1920,4,64]{0,2,1:T(8,128)(2,1)} %bitcast.38, f32[4,384]{1,0:T(4,128)S(1)} %fusion.36, f32[4,1920]{1,0:T(4,128)S(1)} %bitcast.45, f32[4,384]{1,0:T(4,128)S(1)} %bitcast.43, pred[384,1920]{0,1:T(8,128)(4,1)} %compare_and_fusion, bf16[1920,4,64]{0,2,1:T(8,128)(2,1)S(1)} %bitcast.37, ...), kind=kOutput, calls=%fused_computation.23 | convolution fusion | flops 775720320 | bytes 3139584 | tf_op jit(solution)/shard_map/hqk,khd->qhd/dot_general | solution.py:124
  115.2 1.8 convolution_convert_fusion.1
  117.0 14.1 %all-to-all-start = ((bf16[8,48,2048]{2,1,0:T(8,128)(2,1)}), bf16[8,48,2048]{2,1,0:T(8,128)(2,1)S(1)}, u32[]{:S(2)}, u32[]{:S(2)}) async-start(bf16[8,48,2048]{2,1,0:T(8,128)(2,1)} %bitcast.32), calls=%async_computation | async-start | bytes 3145728 | tf_op jit(solution)/shard_map/all_to_all | solution.py:29
  131.1 20.6 %all-to-all-done = bf16[8,48,2048]{2,1,0:T(8,128)(2,1)S(1)} async-done(((bf16[8,48,2048]{2,1,0:T(8,128)(2,1)}), bf16[8,48,2048]{2,1,0:T(8,128)(2,1)S(1)}, u32[]{:S(2)}, u32[]{:S(2)}) %all-to-all-start) | async-done | bytes 1572896 | tf_op jit(solution)/shard_map/all_to_all | solution.py:29
  151.9 1.1 fusion.24
  153.4 24.0 %all_to_all.15 = bf16[8,48,2048]{2,1,0:T(8,128)(2,1)S(1)} all-to-all(bf16[8,48,2048]{2,1,0:T(8,128)(2,1)S(1)} %broadcast_in_dim.16), channel_id=1, replica_groups=mesh['sp_0'=16,'sp_1'=4,'tp'=8] {'tp'}, dimensions={0} | all-to-all | bytes 3145728 | tf_op jit(solution)/shard_map/all_to_all | solution.py:41
  177.3 4.1 %fusion.10 = f32[384,640]{1,0:T(8,128)} fusion(bf16[384,2048]{1,0:T(8,128)(2,1)S(1)} %bitcast.33, bf16[2048,1280]{1,0:T(8,128)(2,1)} %all-gather.3.cloned.1.call-done), kind=kOutput, calls=%fused_computation.18 | convolution fusion | flops 1006632960 | bytes 5177344 | tf_op jit(solution)/shard_map/dot_general | solution.py:137
  181.4 44.6 %all-gather.5.cloned.1.call-done = bf16[640,2048]{0,1:T(8,128)(2,1)} async-done(((bf16[640,128]{0,1:T(8,128)(2,1)}), bf16[640,2048]{0,1:T(8,128)(2,1)}) %all-gather.5.cloned.1.call-update) | async-done | bytes 2621456 | tf_op jit(solution)/shard_map/all_gather | solution.py:61
  226.0 7.1 %convolution_convert_fusion = bf16[384,2048]{1,0:T(8,128)(2,1)} fusion(bf16[640,2048]{0,1:T(8,128)(2,1)} %all-gather.5.cloned.1.call-done, bf16[384,2048]{1,0:T(8,128)(2,1)S(1)} %bitcast.34, bf16[2048,1280]{1,0:T(8,128)(2,1)} %all-gather.3.cloned.1.call-done, f32[384,640]{1,0:T(8,128)} %fusion.10), kind=kOutput, calls=%fused_computation.14 | convolution fusion | flops 2015526912 | bytes 9371648 | tf_op jit(solution)/shard_map/dot_general | solution.py:140
  233.1 35.0 %all_to_all.16 = bf16[8,48,2048]{2,1,0:T(8,128)(2,1)S(1)} all-to-all(bf16[8,48,2048]{2,1,0:T(8,128)(2,1)} %bitcast.35), channel_id=1, replica_groups=mesh['sp_0'=16,'sp_1'=4,'tp'=8] {'tp'}, dimensions={0} | all-to-all | bytes 3145728 | tf_op jit(solution)/shard_map/all_to_all | solution.py:29
  (62 shorter events, 10.5 us)
Async XLA Ops:
  6.5 108.6 %copy-start = (bf16[256,2048]{1,0:T(8,128)(2,1)S(1)}, bf16[256,2048]{1,0:T(8,128)(2,1)}, u32[]{:S(2)}) copy-start(bf16[256,2048]{1,0:T(8,128)(2,1)} %param.17) | copy-start | bytes 3145732
  6.5 87.8 %copy-start.1 = (bf16[384,256]{1,0:T(8,128)(2,1)S(1)}, bf16[384,256]{1,0:T(8,128)(2,1)}, u32[]{:S(2)}) copy-start(bf16[384,256]{1,0:T(8,128)(2,1)} %param.13) | copy-start | bytes 589828
  6.5 88.6 %copy-start.4 = (f32[384,4]{0,1:T(4,128)S(1)}, f32[384,4]{0,1:T(4,128)}, u32[]{:S(2)}) copy-start(f32[384,4]{0,1:T(4,128)} %param.15) | copy-start | bytes 18436
  6.5 170.8 %all-gather.3.cloned.1.call-start = ((), (), s32[]{:S(2)}) async-start(), calls=%async_computation.3 | async-start | bytes 5324800 | tf_op jit(solution)/shard_map/all_gather | solution.py:52
  8.1 217.9 %all-gather.5.cloned.1.call-start = ((), (), s32[]{:S(2)}) async-start(), calls=%async_computation.4 | async-start | bytes 2785280 | tf_op jit(solution)/shard_map/all_gather | solution.py:61
  8.2 33.7 %collective-permute-start.4 = (s32[384]{0:T(512)}, s32[384]{0:T(512)S(1)}, u32[]{:S(2)}, u32[]{:S(2)}) collective-permute-start(s32[384]{0:T(512)} %param.16), channel_id=1, source_target_pairs={{0,32},{8,40},{16,48},{24,56},{32,64},{40,72},{48,80},{56,88},{64,... | collective-permute-start | bytes 4616 | tf_op jit(solution)/shard_map/ppermute | solution.py:19
  12.5 32.9 %collective-permute-start.5 = (s32[384]{0:T(512)}, s32[384]{0:T(512)S(1)}, u32[]{:S(2)}, u32[]{:S(2)}) collective-permute-start(s32[384]{0:T(512)} %param.16), channel_id=1, source_target_pairs={{0,24},{8,32},{16,40},{24,48},{32,56},{40,64},{48,72},{56,80},{64,... | collective-permute-start | bytes 4616 | tf_op jit(solution)/shard_map/ppermute | solution.py:19
  17.2 32.2 %collective-permute-start.6 = (s32[384]{0:T(512)}, s32[384]{0:T(512)S(1)}, u32[]{:S(2)}, u32[]{:S(2)}) collective-permute-start(s32[384]{0:T(512)} %param.16), channel_id=1, source_target_pairs={{0,16},{8,24},{16,32},{24,40},{32,48},{40,56},{48,64},{56,72},{64,... | collective-permute-start | bytes 4616 | tf_op jit(solution)/shard_map/ppermute | solution.py:19
  20.8 30.4 %collective-permute-start.7 = (s32[384]{0:T(512)}, s32[384]{0:T(512)S(1)}, u32[]{:S(2)}, u32[]{:S(2)}) collective-permute-start(s32[384]{0:T(512)} %param.16), channel_id=1, source_target_pairs={{0,8},{8,16},{16,24},{24,32},{32,40},{40,48},{48,56},{56,64},{64,7... | collective-permute-start | bytes 4616 | tf_op jit(solution)/shard_map/ppermute | solution.py:19
  23.4 62.5 %collective-permute-start.8 = (bf16[384,256]{1,0:T(8,128)(2,1)}, bf16[384,256]{1,0:T(8,128)(2,1)S(1)}, u32[]{:S(2)}, u32[]{:S(2)}) collective-permute-start(bf16[384,256]{1,0:T(8,128)(2,1)} %param.13), channel_id=1, source_target_pairs={{0,32},{8,40},{16,48},{24,56},{32,64},{40,72},{48,80},{56,88},{64,... | collective-permute-start | bytes 589832 | tf_op jit(solution)/shard_map/ppermute | solution.py:19
  41.9 46.8 %collective-permute-start.9 = (bf16[384,256]{1,0:T(8,128)(2,1)}, bf16[384,256]{1,0:T(8,128)(2,1)S(1)}, u32[]{:S(2)}, u32[]{:S(2)}) collective-permute-start(bf16[384,256]{1,0:T(8,128)(2,1)} %param.13), channel_id=1, source_target_pairs={{0,24},{8,32},{16,40},{24,48},{32,56},{40,64},{48,72},{56,80},{64,... | collective-permute-start | bytes 589832 | tf_op jit(solution)/shard_map/ppermute | solution.py:19
  45.5 46.8 %collective-permute-start.10 = (bf16[384,256]{1,0:T(8,128)(2,1)}, bf16[384,256]{1,0:T(8,128)(2,1)S(1)}, u32[]{:S(2)}, u32[]{:S(2)}) collective-permute-start(bf16[384,256]{1,0:T(8,128)(2,1)} %param.13), channel_id=1, source_target_pairs={{0,16},{8,24},{16,32},{24,40},{32,48},{40,56},{48,64},{56,72},{64,... | collective-permute-start | bytes 589832 | tf_op jit(solution)/shard_map/ppermute | solution.py:19
  49.4 44.9 %collective-permute-start.11 = (bf16[384,256]{1,0:T(8,128)(2,1)}, bf16[384,256]{1,0:T(8,128)(2,1)S(1)}, u32[]{:S(2)}, u32[]{:S(2)}) collective-permute-start(bf16[384,256]{1,0:T(8,128)(2,1)} %param.13), channel_id=1, source_target_pairs={{0,8},{8,16},{16,24},{24,32},{32,40},{40,48},{48,56},{56,64},{64,7... | collective-permute-start | bytes 589832 | tf_op jit(solution)/shard_map/ppermute | solution.py:19
  51.2 7.6 %collective-permute-start.12 = (f32[384,4]{0,1:T(4,128)}, f32[384,4]{0,1:T(4,128)S(1)}, u32[]{:S(2)}, u32[]{:S(2)}) collective-permute-start(f32[384,4]{0,1:T(4,128)} %param.15), channel_id=1, source_target_pairs={{0,32},{8,40},{16,48},{24,56},{32,64},{40,72},{48,80},{56,88},{64,... | collective-permute-start | bytes 18440 | tf_op jit(solution)/shard_map/ppermute | solution.py:19
  58.8 6.5 %collective-permute-start.13 = (f32[384,4]{0,1:T(4,128)}, f32[384,4]{0,1:T(4,128)S(1)}, u32[]{:S(2)}, u32[]{:S(2)}) collective-permute-start(f32[384,4]{0,1:T(4,128)} %param.15), channel_id=1, source_target_pairs={{0,24},{8,32},{16,40},{24,48},{32,56},{40,64},{48,72},{56,80},{64,... | collective-permute-start | bytes 18440 | tf_op jit(solution)/shard_map/ppermute | solution.py:19
  65.3 4.1 %collective-permute-start.14 = (f32[384,4]{0,1:T(4,128)}, f32[384,4]{0,1:T(4,128)S(1)}, u32[]{:S(2)}, u32[]{:S(2)}) collective-permute-start(f32[384,4]{0,1:T(4,128)} %param.15), channel_id=1, source_target_pairs={{0,16},{8,24},{16,32},{24,40},{32,48},{40,56},{48,64},{56,72},{64,... | collective-permute-start | bytes 18440 | tf_op jit(solution)/shard_map/ppermute | solution.py:19
  69.4 5.7 %collective-permute-start.15 = (f32[384,4]{0,1:T(4,128)}, f32[384,4]{0,1:T(4,128)S(1)}, u32[]{:S(2)}, u32[]{:S(2)}) collective-permute-start(f32[384,4]{0,1:T(4,128)} %param.15), channel_id=1, source_target_pairs={{0,8},{8,16},{16,24},{24,32},{32,40},{40,48},{48,56},{56,64},{64,7... | collective-permute-start | bytes 18440 | tf_op jit(solution)/shard_map/ppermute | solution.py:19
  75.1 27.1 %collective-permute-start = (bf16[384,256]{1,0:T(8,128)(2,1)}, bf16[384,256]{1,0:T(8,128)(2,1)}, u32[]{:S(2)}, u32[]{:S(2)}) collective-permute-start(bf16[384,256]{1,0:T(8,128)(2,1)} %param.14), channel_id=1, source_target_pairs={{0,32},{8,40},{16,48},{24,56},{32,64},{40,72},{48,80},{56,88},{64,... | collective-permute-start | bytes 589832 | tf_op jit(solution)/shard_map/ppermute | solution.py:19
  85.9 17.2 %collective-permute-start.1 = (bf16[384,256]{1,0:T(8,128)(2,1)}, bf16[384,256]{1,0:T(8,128)(2,1)}, u32[]{:S(2)}, u32[]{:S(2)}) collective-permute-start(bf16[384,256]{1,0:T(8,128)(2,1)} %param.14), channel_id=1, source_target_pairs={{0,24},{8,32},{16,40},{24,48},{32,56},{40,64},{48,72},{56,80},{64,... | collective-permute-start | bytes 589832 | tf_op jit(solution)/shard_map/ppermute | solution.py:19
  88.7 15.4 %collective-permute-start.2 = (bf16[384,256]{1,0:T(8,128)(2,1)}, bf16[384,256]{1,0:T(8,128)(2,1)}, u32[]{:S(2)}, u32[]{:S(2)}) collective-permute-start(bf16[384,256]{1,0:T(8,128)(2,1)} %param.14), channel_id=1, source_target_pairs={{0,16},{8,24},{16,32},{24,40},{32,48},{40,56},{48,64},{56,72},{64,... | collective-permute-start | bytes 589832 | tf_op jit(solution)/shard_map/ppermute | solution.py:19
  92.3 12.7 %collective-permute-start.3 = (bf16[384,256]{1,0:T(8,128)(2,1)}, bf16[384,256]{1,0:T(8,128)(2,1)}, u32[]{:S(2)}, u32[]{:S(2)}) collective-permute-start(bf16[384,256]{1,0:T(8,128)(2,1)} %param.14), channel_id=1, source_target_pairs={{0,8},{8,16},{16,24},{24,32},{32,40},{40,48},{48,56},{56,64},{64,7... | collective-permute-start | bytes 589832 | tf_op jit(solution)/shard_map/ppermute | solution.py:19
  95.1 10.8 %copy-start.2 = (bf16[384,256]{1,0:T(8,128)(2,1)S(1)}, bf16[384,256]{1,0:T(8,128)(2,1)}, u32[]{:S(2)}) copy-start(bf16[384,256]{1,0:T(8,128)(2,1)} %param.14) | copy-start | bytes 589828
  117.0 36.0 %copy-start.3 = (f32[2048]{0:T(1024)S(1)}, f32[2048]{0:T(1024)}, u32[]{:S(2)}) copy-start(f32[2048]{0:T(1024)} %param.18) | copy-start | bytes 24580
  117.0 34.7 %all-to-all-start = ((bf16[8,48,2048]{2,1,0:T(8,128)(2,1)}), bf16[8,48,2048]{2,1,0:T(8,128)(2,1)S(1)}, u32[]{:S(2)}, u32[]{:S(2)}) async-start(bf16[8,48,2048]{2,1,0:T(8,128)(2,1)} %bitcast.32), calls=%async_computation | async-start | bytes 3145728 | tf_op jit(solution)/shard_map/all_to_all | solution.py:29
Sparse Core Ops, SparseCore 0:
  10.3 147.4 all-gather.2
  159.9 66.0 all-gather.4
where the time goes:
time: 277 us; the launch traced here: 276 us
  starting transfers between devices  77.6 us (28%)
  blocking collectives  72.6 us (26%)
  waiting for transfers between devices  68.1 us (25%)
  matrix products  27.8 us (10%)
  between operations  13.8 us (5%)
  local copies, waits for them, and re-layouts  8.74 us (3%)
  other arithmetic  7.21 us (3%)
    ppermute x16, starting transfers between devices, from_behind(): lax.ppermute(value, axis, [(source, source + steps) for source in range(f...  63.5 us
    all_gather x1, waiting for transfers between devices, whole_of(): shard = lax.all_gather(shard, axis, axis=dim, tiled=True)  44.6 us
    all_to_all x1, blocking collectives, sent_and_summed(): lax.all_to_all(pieces, axis, split_axis=0, concat_axis=0, tiled=True)  35 us
    all_to_all x1, blocking collectives, copy_for_each(): lax.all_to_all(jnp.broadcast_to(shard[None], (size, *shard.shape)), axis,...  24 us
    all_to_all x1, waiting for transfers between devices, sent_and_summed(): lax.all_to_all(pieces, axis, split_axis=0, concat_axis=0, tiled=True)  20.6 us
    all_to_all x1, starting transfers between devices, sent_and_summed(): lax.all_to_all(pieces, axis, split_axis=0, concat_axis=0, tiled=True)  14.1 us
    all_gather x1, blocking collectives, whole_of(): shard = lax.all_gather(shard, axis, axis=dim, tiled=True)  13.7 us
    dot_general x1, matrix products, local(): jnp.einsum('hqk,khd->qhd', weights, value_heads, preferred_element_type=j...  7.74 us
  transfers between devices with their start and end apart: 19, of which 5 were waited for; matrix products, arithmetic and copies ran while one was open for 12% of the time, Pallas kernels for 0%

commit v1 on v0

v1 whole, which is shorter than its diff:
```python
import functools
import math

import jax
import jax.numpy as jnp
from jax import lax
from jax.experimental import pallas as pl
from jax.experimental.pallas import tpu as pltpu
from jax.sharding import PartitionSpec as P

MESH = pl.DeviceIdType.MESH
EPSILON = 1e-06
NEGATIVE = -1e30
REACH = 4
NY = 4
LOG2E = math.log2(math.e)
F32 = jnp.float32
BF16 = jnp.bfloat16


def dot(a, b):
    return lax.dot_general(a, b, (((1,), (0,)), ((), ())), preferred_element_type=F32)


def dot_nt(a, b):
    return lax.dot_general(a, b, (((1,), (1,)), ((), ())), preferred_element_type=F32)


def kernel(
    n_sp, n_tp,
    q_ref, k_ref, v_ref, aux_ref, gu_ref, dt_ref, wo_ref, res_ref, gain_ref,
    out_ref,
    k_all, v_all, aux_all, gu, dt, wo, res, bias, att, part1, part2, pair1, pair2,
    stage, own, half1, half2, rs1, rs2, x_all, hidden, middle,
    loc, kv_s, kv_r, gz_s, gz_r, gy_s, gy_r, dy_s, dy_r, dz_s, dz_r, rs_s, rs_r, ag_s, ag_r,
):
    nz = n_sp // NY
    nx = n_tp // 2
    hz = nz // 2
    sp, tp = lax.axis_index("sp"), lax.axis_index("tp")
    z, y = sp // NY, sp % NY
    x, c = tp // 2, tp % 2
    tok, width = q_ref.shape
    heads = 4
    rows = tok // n_tp
    d_model = wo.shape[1]
    half = d_model // 2

    def at_sp(dz, dy):
        return ((z + dz + nz) % nz) * NY + (y + dy + NY) % NY

    def at_tp(dx, dc):
        return ((x + dx + nx) % nx) * 2 + (c + dc) % 2

    dev_z = ((at_sp(1, 0), tp), (at_sp(-1, 0), tp))
    dev_y = ((at_sp(0, 1), tp), (at_sp(0, -1), tp), (at_sp(0, 2), tp))
    dev_c = (sp, at_tp(0, 1))
    dev_x = ((sp, at_tp(1, 0)), (sp, at_tp(-1, 0)))

    def remote(src, dst, ssem, rsem, dev):
        return pltpu.make_async_remote_copy(
            src_ref=src, dst_ref=dst, send_sem=ssem, recv_sem=rsem, device_id=dev, device_id_type=MESH
        )

    last = REACH * tok
    local = [
        pltpu.make_async_copy(k_ref, k_all.at[pl.ds(last, tok)], loc.at[0]),
        pltpu.make_async_copy(v_ref, v_all.at[pl.ds(last, tok)], loc.at[1]),
        pltpu.make_async_copy(aux_ref, aux_all.at[:, pl.ds(last, tok)], loc.at[2]),
        pltpu.make_async_copy(gu_ref, gu.at[sp], loc.at[3]),
        pltpu.make_async_copy(dt_ref, dt.at[sp], loc.at[4]),
        pltpu.make_async_copy(wo_ref, wo, loc.at[5]),
        pltpu.make_async_copy(res_ref.at[pl.ds(pl.multiple_of(tp * rows, rows), rows)], res, loc.at[6]),
    ]
    for copy in local:
        copy.start()

    barrier = pltpu.get_barrier_semaphore()
    peers = (*dev_z, *dev_y, dev_c, *dev_x)
    for peer in peers:
        pl.semaphore_signal(barrier, inc=1, device_id=peer, device_id_type=MESH)
    pl.semaphore_wait(barrier, len(peers))

    def kv_slot(item, offset):
        if item == 2:
            return aux_all.at[:, pl.ds(pl.multiple_of(offset, 128), tok)]
        return (k_all, v_all)[item].at[pl.ds(pl.multiple_of(offset, 128), tok)]

    def kv_copy(item, kind, src, distance, dev):
        return remote(
            kv_slot(item, src), kv_slot(item, (REACH - distance) * tok),
            kv_s.at[item, kind], kv_r.at[item, distance - 1], dev,
        )

    def kv_prev(item):
        return kv_copy(item, 0, last, 4, dev_z[0])

    def kv_right(item, src):
        return kv_copy(item, 1, src, 1, dev_y[0])

    def kv_left(item, src):
        return kv_copy(item, 2, src, 3, dev_y[1])

    def kv_relay_right(item):
        return kv_copy(item, 3, (REACH - 1) * tok, 2, dev_y[0])

    def kv_relay_left(item):
        return kv_copy(item, 4, (REACH - 3) * tok, 2, dev_y[1])

    ITEMS = (2, 0, 1)
    for item in (2, 0, 1):
        local[item].wait()
        kv_prev(item).start()

        @pl.when(y < NY - 1)
        def _():
            kv_right(item, last).start()

        @pl.when(y == 0)
        def _():
            kv_left(item, last).start()

    def z_copy(way, r):
        shard = at_sp(-r, 0) if way == 0 else at_sp(r, 0)
        return remote(gu.at[shard], gu.at[shard], gz_s.at[way, r + 1], gz_r.at[way, r + 1], dev_z[way])

    def z_arrival(way, r):
        shard = at_sp(-r, 0) if way == 0 else at_sp(r, 0)
        return remote(gu.at[shard], gu.at[shard], gz_s.at[way, r], gz_r.at[way, r], dev_z[way])

    def y_copy(way, o):
        shard, plane = at_sp(o, 0), (o + nz) % nz
        return remote(gu.at[shard], gu.at[shard], gy_s.at[way, plane], gy_r.at[way, plane], dev_y[way])

    def y_arrival(way, o):
        shard, plane = at_sp(o, -1 if way == 0 else 1), (o + nz) % nz
        return remote(gu.at[shard], gu.at[shard], gy_s.at[way, plane], gy_r.at[way, plane], dev_y[way])

    def y_forward(way, o):
        shard, plane = at_sp(o, -1 if way == 0 else 1), (o + nz) % nz
        return remote(gu.at[shard], gu.at[shard], gy_s.at[2, plane], gy_r.at[2, plane], dev_y[way])

    def y_across(o):
        shard, plane = at_sp(o, 2), (o + nz) % nz
        return remote(gu.at[shard], gu.at[shard], gy_s.at[2, plane], gy_r.at[2, plane], dev_y[0])

    def d_copy(i):
        return remote(dt.at[sp], dt.at[sp], dy_s.at[i], dy_r.at[i], dev_y[i])

    def d_arrival(i):
        shard = at_sp(0, (-1, 1, 2)[i])
        return remote(dt.at[shard], dt.at[shard], dy_s.at[i], dy_r.at[i], dev_y[i])

    def q_ref_of(way, r):
        plane = (z + (-r if way == 0 else r) + nz) % nz
        return dt.at[pl.ds(plane * NY, NY)]

    def q_copy(way, r):
        block = q_ref_of(way, r)
        return remote(block, block, dz_s.at[way, r + 1], dz_r.at[way, r + 1], dev_z[way])

    def q_arrival(way, r):
        block = q_ref_of(way, r)
        return remote(block, block, dz_s.at[way, r], dz_r.at[way, r], dev_z[way])

    def z_round(r, at_end=0):
        z_arrival(0, r).wait_recv()
        if at_end < 2:
            z_copy(0, r).start()
        y_copy(0, -r).start()
        y_copy(1, -r).start()
        if at_end < 2:
            z_arrival(1, r).wait_recv()
            if at_end < 1:
                z_copy(1, r).start()
            y_copy(0, r).start()
            y_copy(1, r).start()

    def y_round(r, at_end=0):
        if at_end < 2:
            y_arrival(1, r).wait_recv()
            y_forward(1, r).start()
        if not (isinstance(r, int) and r == 0):
            y_arrival(0, -r).wait_recv()
            y_forward(0, -r).start()

    def q_round(r, at_end=0):
        q_arrival(0, r).wait_recv()
        if at_end < 2:
            q_copy(0, r).start()
            q_arrival(1, r).wait_recv()
            if at_end < 1:
                q_copy(1, r).start()

    def stage_of(r):
        return 2 if r == hz else 1 if r == hz - 1 else 0

    def full_round(r):
        z_round(r, stage_of(r))
        y_round(r - 1, stage_of(r - 1))
        q_round(r, stage_of(r))

    local[3].wait()
    z_copy(0, 0).start()
    z_copy(1, 0).start()
    y_copy(0, 0).start()
    y_copy(1, 0).start()
    local[4].wait()
    for i in range(3):
        d_copy(i).start()

    for item in ITEMS:
        kv_copy(item, 0, last, 4, dev_z[0]).wait_recv()

        @pl.when(y == NY - 1)
        def _():
            kv_right(item, 0).start()

        @pl.when(y > 0)
        def _():
            kv_left(item, 0).start()

    for i in range(3):
        d_arrival(i).wait_recv()
    q_copy(0, 0).start()
    q_copy(1, 0).start()

    for item in ITEMS:
        kv_right(item, last).wait_recv()

        @pl.when((y == 1) | (y == 2))
        def _():
            kv_relay_right(item).start()

        kv_left(item, last).wait_recv()

        @pl.when((y == 1) | (y == 2))
        def _():
            kv_relay_left(item).start()

    full_round(1)
    for item in ITEMS:
        kv_relay_right(item).wait_recv()

    tile = 128 if tok % 128 == 0 else tok
    window = REACH * tok + tile
    lanes = lax.broadcasted_iota(jnp.int32, (1, width), 1) // (width // heads)
    scale = (width // heads) ** -0.5 * LOG2E
    own_docs = jnp.transpose(aux_all[:, pl.ds(last, tok)], (1, 0))
    att_docs = own_docs[:, heads : heads + 1]
    origin = own_docs[0:1, 0:heads]
    half1[...] = jnp.broadcast_to(att_docs, half1.shape)

    def attend(i, carry):
        start = pl.multiple_of(i * tile, tile)
        doc_row = aux_all[heads : heads + 1, pl.ds(start, window)]
        doc_col = half1[pl.ds(start, tile), 0:1]
        gap = lax.broadcasted_iota(jnp.int32, (tile, window), 1) - lax.broadcasted_iota(jnp.int32, (tile, window), 0)
        bias[...] = jnp.where((doc_row == doc_col) & (gap <= REACH * tok), 0.0, NEGATIVE)
        queries = q_ref[pl.ds(start, tile), :]
        keys = k_all[pl.ds(start, window), :]
        values = v_all[pl.ds(start, window), :]
        total = jnp.zeros((tile, width), F32)
        for h in range(heads):
            masked = jnp.where(lanes == h, queries, jnp.zeros_like(queries))
            gates = (origin[:, h : h + 1] - aux_all[h : h + 1, pl.ds(start, window)]) * LOG2E
            scores = dot_nt(masked, keys) * scale + gates + bias[...]
            peak = jnp.max(scores, axis=-1, keepdims=True)
            weights = jnp.exp2(scores - peak)
            norm = jnp.sum(weights, axis=-1, keepdims=True)
            mixed = dot(weights.astype(BF16), values)
            total = jnp.where(lanes == h, mixed / norm, total)
        att[pl.ds(start, tile), :] = total.astype(BF16)
        r = i + 2
        z_round(r)
        y_round(r - 1)
        q_round(r)
        return carry

    n_tiles = tok // tile
    lax.fori_loop(0, n_tiles, attend, 0)
    rounds = [functools.partial(full_round, r) for r in range(n_tiles + 2, hz + 1)]

    def serve():
        if rounds:
            rounds.pop(0)()

    n_tile = 256

    def summed(part, pair, half_in, rs_in, k, service):
        swap = remote(part.at[:, 1 - c], pair, rs_s.at[k, 0], rs_r.at[k, 0], dev_c)
        swap.start()
        service()
        swap.wait_recv()

        def on_chip(there):
            return part[there, c].astype(F32) + pair[there].astype(F32)

        far, right, left = (x + 2) % nx, (x + 1) % nx, (x + nx - 1) % nx
        lo, hi = pl.ds(0, half), pl.ds(half, half)
        total = on_chip(far).astype(BF16)
        stage[k, 0] = total[:, :half]
        stage[k, 1] = total[:, half:]
        first = [
            remote(stage.at[k, 0], half_in.at[0], rs_s.at[k, 1], rs_r.at[k, 1], dev_x[0]),
            remote(stage.at[k, 1], half_in.at[1], rs_s.at[k, 2], rs_r.at[k, 2], dev_x[1]),
        ]
        first[0].start()
        first[1].start()
        to_right = on_chip(right)
        to_left = on_chip(left)
        stage[k, 2] = to_right[:, half:].astype(BF16)
        stage[k, 3] = to_left[:, :half].astype(BF16)
        second = [
            remote(stage.at[k, 2], rs_in.at[0, 1], rs_s.at[k, 3], rs_r.at[k, 3], dev_x[0]),
            remote(stage.at[k, 3], rs_in.at[1, 0], rs_s.at[k, 4], rs_r.at[k, 4], dev_x[1]),
        ]
        second[0].start()
        second[1].start()
        own[...] = on_chip(x)
        service()
        first[0].wait_recv()
        stage[k, 4] = (to_right[:, :half] + half_in[0].astype(F32)).astype(BF16)
        third = remote(stage.at[k, 4], rs_in.at[0, 0], rs_s.at[k, 5], rs_r.at[k, 5], dev_x[0])
        third.start()
        first[1].wait_recv()
        stage[k, 5] = (to_left[:, half:] + half_in[1].astype(F32)).astype(BF16)
        fourth = remote(stage.at[k, 5], rs_in.at[1, 1], rs_s.at[k, 6], rs_r.at[k, 6], dev_x[1])
        fourth.start()
        for copy in (*second, third, fourth):
            copy.wait_recv()
        sends = (swap, *first, *second, third, fourth)
        halves = [
            own[:, i * half : (i + 1) * half] + rs_in[0, i].astype(F32) + rs_in[1, i].astype(F32) for i in range(2)
        ]
        return jnp.concatenate(halves, axis=-1), sends

    local[5].wait()
    attended = att[...]

    def project(n, carry):
        cols = pl.ds(pl.multiple_of(n * n_tile, n_tile), n_tile)
        product = dot(attended, wo[:, cols]).astype(BF16)
        part1[:, :, :, cols] = product.reshape(nx, 2, rows, n_tile)
        return carry

    lax.fori_loop(0, d_model // n_tile, project, 0)
    attn_sum, sends1 = summed(part1, pair1, half2.at[0], rs1, 0, serve)
    local[6].wait()
    mid = (res[...].astype(F32) + attn_sum).astype(BF16)
    middle[...] = mid
    wide = mid.astype(F32)
    factor = lax.rsqrt(jnp.mean(wide * wide, axis=-1, keepdims=True) + EPSILON)
    x_all[tp] = (wide * factor * gain_ref[...]).astype(BF16)

    def ag(slot, cols, i, dev):
        ref = x_all.at[slot] if cols is None else x_all.at[slot, :, cols]
        return remote(ref, ref, ag_s.at[i], ag_r.at[i], dev)

    lo, hi = pl.ds(0, half), pl.ds(half, half)
    sends2 = [ag(tp, None, 0, dev_x[0]), ag(tp, None, 1, dev_x[1]), ag(tp, None, 4, dev_c)]
    for copy in sends2:
        copy.start()
    serve()
    from_left, from_right, from_far = at_tp(-1, 0), at_tp(1, 0), at_tp(2, 0)
    ag(from_left, None, 0, dev_x[0]).wait_recv()
    more = [ag(from_left, lo, 2, dev_x[0]), ag(from_left, None, 5, dev_c)]
    for copy in more:
        copy.start()
    sends2 += more
    ag(from_right, None, 1, dev_x[1]).wait_recv()
    more = [ag(from_right, hi, 3, dev_x[1]), ag(from_right, None, 6, dev_c)]
    for copy in more:
        copy.start()
    sends2 += more
    ag(from_far, lo, 2, dev_x[0]).wait_recv()
    ag(from_far, hi, 3, dev_x[1]).wait_recv()
    copy = ag(from_far, None, 7, dev_c)
    copy.start()
    sends2.append(copy)
    while rounds:
        serve()
    y_round(hz, 2)
    ag(at_tp(0, 1), None, 4, dev_c).wait_recv()
    ag(at_tp(-1, 1), None, 5, dev_c).wait_recv()
    ag(at_tp(1, 1), None, 6, dev_c).wait_recv()
    ag(at_tp(2, 1), None, 7, dev_c).wait_recv()

    def rest(o, carry):
        y_arrival(0, o).wait_recv()
        y_across(o).wait_recv()
        y_arrival(1, o - hz).wait_recv()
        y_across(o - hz).wait_recv()
        return carry

    lax.fori_loop(0, hz, rest, 0)

    ff = hidden.shape[1]

    def expand(n, carry):
        cols = pl.ds(pl.multiple_of(n * 256, 256), 256)
        both = dot(x_all[...].reshape(tok, d_model), gu[:, :, cols].reshape(d_model, 256))
        gate, up = both[:, :128], both[:, 128:]
        act = gate / (1.0 + jnp.exp(-gate)) * up
        hidden[:, pl.ds(pl.multiple_of(n * 128, 128), 128)] = act.astype(BF16)
        return carry

    lax.fori_loop(0, ff // 128, expand, 0)
    group = n_tile // (d_model // n_sp)

    def contract(n, carry):
        cols = pl.ds(pl.multiple_of(n * n_tile, n_tile), n_tile)
        block = dt[pl.ds(n * group, group)].reshape(n_tile, ff)
        product = dot_nt(hidden[...], block).astype(BF16)
        part2[:, :, :, cols] = product.reshape(nx, 2, rows, n_tile)
        return carry

    lax.fori_loop(0, d_model // n_tile, contract, 0)
    down_sum, sends3 = summed(part2, pair2, half2.at[1], rs2, 1, lambda: None)
    out_ref[...] = (middle[...].astype(F32) + down_sum).astype(BF16)

    for copy in (*sends1, *sends2, *sends3):
        copy.wait_send()
    for item in ITEMS:
        kv_prev(item).wait_send()
        kv_right(item, last).wait_send()
        kv_left(item, last).wait_send()

        @pl.when((y == 1) | (y == 2))
        def _():
            kv_relay_right(item).wait_send()
            kv_relay_left(item).wait_send()

    for i in range(3):
        d_copy(i).wait_send()

    def gone_z(r, carry):
        for way in range(2):
            z_copy(way, r).wait_send()
            q_copy(way, r).wait_send()
        return carry

    lax.fori_loop(0, hz - 1, gone_z, 0)
    z_copy(0, hz - 1).wait_send()
    q_copy(0, hz - 1).wait_send()

    def gone_y(o, carry):
        y_copy(0, o).wait_send()
        y_copy(1, o).wait_send()
        y_across(o).wait_send()
        return carry

    lax.fori_loop(0, nz, gone_y, 0)


def local(n_sp, n_tp, residual, queries, keys, values, gate_cache, doc_ids, out_weight, mix_gain, gate_weight, up_weight, down_weight):
    tok, width = queries.shape
    d_model = out_weight.shape[1]
    rows = tok // n_tp
    wr, ff = gate_weight.shape
    heads = gate_cache.shape[1]
    both = jnp.concatenate(
        [gate_weight.reshape(wr, ff // 128, 1, 128), up_weight.reshape(wr, ff // 128, 1, 128)], axis=2
    ).reshape(wr, 2 * ff)
    down = down_weight.T
    aux = jnp.concatenate(
        [gate_cache.T, doc_ids.astype(F32)[None], jnp.zeros((8 - heads - 1, tok), F32)], axis=0
    )
    nz = n_sp // NY
    hz = nz // 2
    tile = 128 if tok % 128 == 0 else tok
    half = d_model // 2
    vmem = pl.BlockSpec(memory_space=pltpu.VMEM)
    anywhere = pl.BlockSpec(memory_space=pl.ANY)
    dma = pltpu.SemaphoreType.DMA
    return pl.pallas_call(
        functools.partial(kernel, n_sp, n_tp),
        out_shape=jax.ShapeDtypeStruct((rows, d_model), BF16),
        in_specs=[vmem, anywhere, anywhere, anywhere, anywhere, anywhere, anywhere, anywhere, vmem],
        out_specs=vmem,
        scratch_shapes=[
            pltpu.VMEM(((REACH + 1) * tok, width), BF16),
            pltpu.VMEM(((REACH + 1) * tok, width), BF16),
            pltpu.VMEM((8, (REACH + 1) * tok), F32),
            pltpu.VMEM((n_sp, wr, 2 * ff), BF16),
            pltpu.VMEM((n_sp, wr, ff), BF16),
            pltpu.VMEM((width, d_model), BF16),
            pltpu.VMEM((rows, d_model), BF16),
            pltpu.VMEM((tile, REACH * tok + tile), F32),
            pltpu.VMEM((tok, width), BF16),
            pltpu.VMEM((n_tp // 2, 2, rows, d_model), BF16),
            pltpu.VMEM((n_tp // 2, 2, rows, d_model), BF16),
            pltpu.VMEM((n_tp // 2, rows, d_model), BF16),
            pltpu.VMEM((n_tp // 2, rows, d_model), BF16),
            pltpu.VMEM((2, 6, rows, half), BF16),
            pltpu.VMEM((rows, d_model), F32),
            pltpu.VMEM((tok, 128), F32),
            pltpu.VMEM((2, 2, rows, half), BF16),
            pltpu.VMEM((2, 2, rows, half), BF16),
            pltpu.VMEM((2, 2, rows, half), BF16),
            pltpu.VMEM((n_tp, rows, d_model), BF16),
            pltpu.VMEM((tok, ff), BF16),
            pltpu.VMEM((rows, d_model), BF16),
            dma((7,)),
            dma((3, 5)),
            dma((3, 4)),
            dma((2, hz + 1)),
            dma((2, hz + 1)),
            dma((3, nz)),
            dma((3, nz)),
            dma((3,)),
            dma((3,)),
            dma((2, hz + 1)),
            dma((2, hz + 1)),
            dma((2, 7)),
            dma((2, 7)),
            dma((8,)),
            dma((8,)),
        ],
        compiler_params=pltpu.CompilerParams(
            collective_id=0, has_side_effects=True, vmem_limit_bytes=60 * 1024 * 1024
        ),
    )(queries, keys, values, aux, both, down, out_weight, residual, mix_gain[None])


def solution(mesh):
    n_sp, n_tp = mesh.shape["sp"], mesh.shape["tp"]
    return jax.shard_map(
        functools.partial(local, n_sp, n_tp),
        mesh=mesh,
        in_specs=(
            P("sp", None), P("sp", "tp"), P("sp", "tp"), P("sp", "tp"), P("sp", "tp"), P("sp"),
            P("tp", None), P(), P("sp", "tp"), P("sp", "tp"), P("tp", "sp"),
        ),
        out_specs=P(("sp", "tp"), None),
        check_vma=False,
    )
```

time: 277 us -> 115 us (0.42)
  Pallas kernels: 0 us -> 108 us
  starting transfers between devices: 77.6 us -> 0 us
  blocking collectives: 72.6 us -> 0 us
  waiting for transfers between devices: 68.1 us -> 0 us
  matrix products: 27.8 us -> 0 us
  between operations: 13.8 us -> 0.03 us
  other arithmetic: 7.21 us -> 2.07 us
  local copies, waits for them, and re-layouts: 8.74 us -> 4.16 us
    pallas_call x0 -> x1, Pallas kernels: none -> 108 us  [local(): pl.pallas_call(functools.partial(kernel, n_sp, n_tp), out_shape=jax.Shape...]
    ppermute x16 -> x0, starting transfers between devices: 63.5 us -> none  [from_behind(): lax.ppermute(value, axis, [(source, source + steps) for source in range(f...]
    all_to_all x2 -> x0, blocking collectives: 58.9 us -> none  [the longest x1 35 us: sent_and_summed(): lax.all_to_all(pieces, axis, split_axis=0, concat_axis=0, tiled=True)]
    all_gather x2 -> x0, waiting for transfers between devices: 44.6 us -> none  [the longest x1 44.6 us: whole_of(): shard = lax.all_gather(shard, axis, axis=dim, tiled=True)]
    dot_general x4 -> x0, matrix products: 20.8 us -> none  [the longest x1 7.74 us: local(): jnp.einsum('hqk,khd->qhd', weights, value_heads, preferred_element_type=j...]
    all_to_all x1 -> x0, waiting for transfers between devices: 20.6 us -> none  [sent_and_summed(): lax.all_to_all(pieces, axis, split_axis=0, concat_axis=0, tiled=True)]
    all_to_all x1 -> x0, starting transfers between devices: 14.1 us -> none  [sent_and_summed(): lax.all_to_all(pieces, axis, split_axis=0, concat_axis=0, tiled=True)]
    all_gather x1 -> x0, blocking collectives: 13.7 us -> none  [whole_of(): shard = lax.all_gather(shard, axis, axis=dim, tiled=True)]
  transfers between devices with their start and end apart: 19 -> 0, of which waited for: 5 -> 0; matrix products, arithmetic and copies ran while one was open for 12% -> 0% of each run, Pallas kernels for 0% -> 0%
where the time goes in v1:
time: 115 us
  Pallas kernels  108 us (94%)
  local copies, waits for them, and re-layouts  4.16 us (4%)
  other arithmetic  2.07 us (2%)
    pallas_call x1, Pallas kernels, local(): pl.pallas_call(functools.partial(kernel, n_sp, n_tp), out_shape=jax.Shape...  108 us

profile of v1, /device:TPU:1, one launch (start us, length us, event | category | flops | bytes accessed | tf_op | source)
XLA Modules:
  0.0 114.6 jit_solution(11961178444786028909)
XLA Ops:
  0.0 0.1 pad.4.clone
  0.1 0.7 convert_element_type.3
  0.8 1.4 %maximum_maximum_fusion.aux_ref = f32[8,384]{1,0:T(8,128)} fusion(f32[1,384]{1,0:T(1,128)S(1)} %broadcast_in_dim.9, f32[4,384]{1,0:T(4,128)} %bitcast.5, f32[8]{0:T(128)S(1)} %pad.4.clone), kind=kLoop, calls=%fused_computation.1 | loop fusion | flops 6144 | bytes 20000 | tf_op jit(solution)/shard_map/concatenate | solution.py:466
  2.1 0.8 reshape.9
  3.0 0.8 reshape.10
  3.9 0.1 copy.14
  4.0 0.7 reshape.11.gu_ref
  4.6 108.3 %shard_map.109 = bf16[48,2048]{1,0:T(8,128)(2,1)} custom-call(bf16[384,256]{1,0:T(8,128)(2,1)} %q_ref.1, bf16[384,256]{1,0:T(8,128)(2,1)} %k_ref.1, bf16[384,256]{1,0:T(8,128)(2,1)} %v_ref.1, f32[8,384]{1,0:T(8,128)} %maximum_maximum_fusion.aux_ref, bf16[32,1280]{1,0:T(8,128)(2,1)} %reshape.11.gu_ref, bf16[32,640]{1,0:T(8,128)(2,1)} %bitcast.3, ...), custom_call_target="tpu_custom_call" | custom-call | tf_op jit(solution)/shard_map/pallas_call | solution.py:476
  113.0 1.6 %copy.16 = bf16[48,2048]{1,0:T(8,128)(2,1)} copy(bf16[48,2048]{1,0:T(8,128)(2,1)} %shard_map.109) | data formatting | bytes 393216
  (3 shorter events, 0.0 us)

commit v2 on v1

v2 whole, which is shorter than its diff:
```python
import functools
import math

import jax
import jax.numpy as jnp
from jax import lax
from jax.experimental import pallas as pl
from jax.experimental.pallas import tpu as pltpu
from jax.sharding import PartitionSpec as P

MESH = pl.DeviceIdType.MESH
EPSILON = 1e-06
NEGATIVE = -1e30
REACH = 4
NY = 4
LOG2E = math.log2(math.e)
F32 = jnp.float32
BF16 = jnp.bfloat16


def dot(a, b):
    return lax.dot_general(a, b, (((1,), (0,)), ((), ())), preferred_element_type=F32)


def dot_nt(a, b):
    return lax.dot_general(a, b, (((1,), (1,)), ((), ())), preferred_element_type=F32)


def kernel(
    n_sp, n_tp,
    q_ref, k_ref, v_ref, aux_ref, p_ref, d_ref, wo_ref, res_ref, gain_ref,
    out_ref,
    k_all, v_all, aux_all, gu, qd, wo, res, bias, doc_col, att, part, pair,
    stage, own, half_in, rs_in, x_all, hidden, middle,
    loc, kv_s, kv_r, gz_s, gz_r, gy_s, gy_r, dy_s, dy_r, dz_s, dz_r, rs_s, rs_r, wo_s, wo_r, ag_s, ag_r,
):
    nz = n_sp // NY
    nx = n_tp // 2
    hz = nz // 2
    sp, tp = lax.axis_index("sp"), lax.axis_index("tp")
    z, y = sp // NY, sp % NY
    x, c = tp // 2, tp % 2
    tok, width = q_ref.shape
    heads = 4
    rows = tok // n_tp
    d_model = wo.shape[2]
    half = d_model // 2
    ff = hidden.shape[1]
    extra = qd.shape[2] - ff
    tile = 128
    n_tiles = tok // tile

    def at_sp(dz, dy):
        return ((z + dz + nz) % nz) * NY + (y + dy + NY) % NY

    def at_tp(dx, dc):
        return ((x + dx + nx) % nx) * 2 + (c + dc) % 2

    dev_z = ((at_sp(1, 0), tp), (at_sp(-1, 0), tp))
    dev_y = ((at_sp(0, 1), tp), (at_sp(0, -1), tp), (at_sp(0, 2), tp))
    dev_c = (sp, at_tp(0, 1))
    dev_x = ((sp, at_tp(1, 0)), (sp, at_tp(-1, 0)))

    def remote(src, dst, ssem, rsem, dev):
        return pltpu.make_async_remote_copy(
            src_ref=src, dst_ref=dst, send_sem=ssem, recv_sem=rsem, device_id=dev, device_id_type=MESH
        )

    last = REACH * tok
    local = [
        pltpu.make_async_copy(k_ref, k_all.at[pl.ds(last, tok)], loc.at[0]),
        pltpu.make_async_copy(v_ref, v_all.at[pl.ds(last, tok)], loc.at[1]),
        pltpu.make_async_copy(aux_ref, aux_all.at[:, pl.ds(last, tok)], loc.at[2]),
        pltpu.make_async_copy(p_ref, gu.at[sp], loc.at[3]),
        pltpu.make_async_copy(d_ref, qd.at[sp], loc.at[4]),
        pltpu.make_async_copy(wo_ref, wo.at[tp], loc.at[5]),
        pltpu.make_async_copy(res_ref, res, loc.at[6]),
    ]
    for i in (4, 2, 0, 1, 3, 5, 6):
        local[i].start()

    barrier = pltpu.get_barrier_semaphore()
    peers = (*dev_z, *dev_y, dev_c, *dev_x)
    for peer in peers:
        pl.semaphore_signal(barrier, inc=1, device_id=peer, device_id_type=MESH)
    pl.semaphore_wait(barrier, len(peers))

    def kv_slot(item, offset):
        if item == 2:
            return aux_all.at[:, pl.ds(pl.multiple_of(offset, 128), tok)]
        return (k_all, v_all)[item].at[pl.ds(pl.multiple_of(offset, 128), tok)]

    def kv_copy(item, kind, src, distance, dev):
        return remote(
            kv_slot(item, src), kv_slot(item, (REACH - distance) * tok),
            kv_s.at[item, kind], kv_r.at[item, distance - 1], dev,
        )

    def kv_prev(item):
        return kv_copy(item, 0, last, 4, dev_z[0])

    def kv_right(item, src):
        return kv_copy(item, 1, src, 1, dev_y[0])

    def kv_left(item, src):
        return kv_copy(item, 2, src, 3, dev_y[1])

    def kv_relay_right(item):
        return kv_copy(item, 3, (REACH - 1) * tok, 2, dev_y[0])

    def kv_relay_left(item):
        return kv_copy(item, 4, (REACH - 3) * tok, 2, dev_y[1])

    ITEMS = (2, 0, 1)

    def kv_own(item):
        local[item].wait()
        kv_prev(item).start()

        @pl.when(y < NY - 1)
        def _():
            kv_right(item, last).start()

        @pl.when(y == 0)
        def _():
            kv_left(item, last).start()

    def kv_turn(item):
        kv_prev(item).wait_recv()

        @pl.when(y == NY - 1)
        def _():
            kv_right(item, 0).start()

        @pl.when(y > 0)
        def _():
            kv_left(item, 0).start()

    def kv_relay(item):
        kv_right(item, last).wait_recv()

        @pl.when((y == 1) | (y == 2))
        def _():
            kv_relay_right(item).start()

        kv_left(item, last).wait_recv()

        @pl.when((y == 1) | (y == 2))
        def _():
            kv_relay_left(item).start()

    def z_copy(way, r):
        shard = at_sp(-r, 0) if way == 0 else at_sp(r, 0)
        return remote(gu.at[shard], gu.at[shard], gz_s.at[way, r + 1], gz_r.at[way, r + 1], dev_z[way])

    def z_arrival(way, r):
        shard = at_sp(-r, 0) if way == 0 else at_sp(r, 0)
        return remote(gu.at[shard], gu.at[shard], gz_s.at[way, r], gz_r.at[way, r], dev_z[way])

    def y_move(way, o, dy, lane):
        shard, plane = at_sp(o, dy), (o + nz) % nz
        return remote(gu.at[shard], gu.at[shard], gy_s.at[lane, plane], gy_r.at[lane, plane], dev_y[way])

    def y_copy(way, o):
        return y_move(way, o, 0, way)

    def y_arrival(way, o):
        return y_move(way, o, -1 if way == 0 else 1, way)

    def y_forward(way, o):
        return y_move(way, o, -1 if way == 0 else 1, 2)

    def y_across(o):
        return y_move(0, o, 2, 2)

    def d_copy(i):
        return remote(qd.at[sp], qd.at[sp], dy_s.at[i], dy_r.at[i], dev_y[i])

    def d_arrival(i):
        shard = at_sp(0, (-1, 1, 2)[i])
        return remote(qd.at[shard], qd.at[shard], dy_s.at[i], dy_r.at[i], dev_y[i])

    def q_move(way, r, s, step):
        plane = (z + (-r if way == 0 else r) + nz) % nz
        block = qd.at[pl.ds(plane * NY + s * (NY // 2), NY // 2)]
        return remote(block, block, dz_s.at[way, r + step, s], dz_r.at[way, r + step, s], dev_z[way])

    def q_copy(way, r, s):
        return q_move(way, r, s, 1)

    def q_arrival(way, r, s):
        return q_move(way, r, s, 0)

    def pieces(r):
        fixed = isinstance(r, int)

        def along_z():
            for way in range(2):
                count = hz - 1 + way
                if fixed and r > count:
                    continue
                z_arrival(way, r).wait_recv()
                if not fixed or r < count:
                    z_copy(way, r).start()
                for side in range(2):
                    y_copy(side, -r if way == 0 else r).start()

        def bundles(s):
            for way in range(2):
                count = hz - 1 + way
                if fixed and r > count:
                    continue
                q_arrival(way, r, s).wait_recv()
                if not fixed or r < count:
                    q_copy(way, r, s).start()

        def along_y():
            y_turn(r - 1)

        return [along_z, functools.partial(bundles, 0), along_y, functools.partial(bundles, 1)]

    def y_turn(r):
        fixed = isinstance(r, int)
        if not fixed or r < hz:
            y_arrival(0, -r).wait_recv()
            y_forward(0, -r).start()
        if not fixed or r > 0:
            y_arrival(1, r).wait_recv()
            y_forward(1, r).start()

    class Gather:
        def __init__(self, view, send, recv, count):
            self.view, self.send, self.recv, self.count = view, send, recv, count

        def copy(self, kind, slot, j):
            ref = self.view(slot, j, {2: 0, 3: 1}.get(kind))
            dev = dev_c if kind >= 4 else dev_x[kind % 2]
            return remote(ref, ref, self.send.at[kind, j], self.recv.at[kind, j], dev)

        def begin(self, j):
            for kind in (0, 1, 4):
                self.copy(kind, tp, j).start()

        def near(self, j):
            for way in range(2):
                slot = at_tp(2 * way - 1, 0)
                self.copy(way, slot, j).wait_recv()
                self.copy(2 + way, slot, j).start()
                self.copy(5 + way, slot, j).start()

        def far(self, j):
            slot = at_tp(2, 0)
            self.copy(2, slot, j).wait_recv()
            self.copy(3, slot, j).wait_recv()
            self.copy(7, slot, j).start()

        def done(self, j):
            for kind, dx in ((4, 0), (5, -1), (6, 1), (7, 2)):
                self.copy(kind, at_tp(dx, 1), j).wait_recv()

        def gone(self):
            for kind in range(8):
                for j in range(self.count):
                    self.copy(kind, tp, j).wait_send()

    def wo_view(slot, j, part_of):
        size = width // 4
        if part_of is None:
            return wo.at[slot, pl.ds(j * size, size)]
        return wo.at[slot, pl.ds(j * size + part_of * (size // 2), size // 2)]

    def att_view(slot, j, part_of):
        cols = pl.ds(pl.multiple_of(slot * width, 128), width)
        if part_of is None:
            return att.at[pl.ds(pl.multiple_of(j * tile, tile), tile), cols]
        return att.at[pl.ds(pl.multiple_of(j * tile + part_of * (tile // 2), tile // 2), tile // 2), cols]

    wos = Gather(wo_view, wo_s, wo_r, 4)
    ats = Gather(att_view, ag_s, ag_r, n_tiles)

    local[4].wait()
    for i in range(3):
        d_copy(i).start()
    for item in ITEMS:
        kv_own(item)
    local[3].wait()
    z_copy(0, 0).start()
    z_copy(1, 0).start()
    y_copy(0, 0).start()
    y_copy(1, 0).start()
    local[5].wait()
    for j in range(4):
        wos.begin(j)
    for i in range(3):
        d_arrival(i).wait_recv()
    for s in range(2):
        for way in range(2):
            q_copy(way, 0, s).start()
    kv_turn(2)
    kv_turn(0)
    wos.near(0)
    kv_turn(1)
    kv_relay(2)
    kv_relay(0)
    wos.near(1)
    first = pieces(1)
    first[0]()
    kv_relay(1)
    for piece in first[1:]:
        piece()
    wos.near(2)
    for piece in pieces(2):
        piece()
    wos.near(3)
    for item in ITEMS:
        kv_relay_right(item).wait_recv()

    window = REACH * tok + tile
    lanes = lax.broadcasted_iota(jnp.int32, (1, width), 1) // (width // heads)
    scale = (width // heads) ** -0.5 * LOG2E
    own_docs = jnp.transpose(aux_all[:, pl.ds(last, tok)], (1, 0))
    origin = own_docs[0:1, 0:heads]
    doc_col[...] = jnp.broadcast_to(own_docs[:, heads : heads + 1], doc_col.shape)
    own_cols = pl.ds(pl.multiple_of(tp * width, 128), width)

    def attend(i, carry):
        start = pl.multiple_of(i * tile, tile)
        doc_row = aux_all[heads : heads + 1, pl.ds(start, window)]
        doc_here = doc_col[pl.ds(start, tile), 0:1]
        gap = lax.broadcasted_iota(jnp.int32, (tile, window), 1) - lax.broadcasted_iota(jnp.int32, (tile, window), 0)
        bias[...] = jnp.where((doc_row == doc_here) & (gap <= REACH * tok), 0.0, NEGATIVE)
        queries = q_ref[pl.ds(start, tile), :]
        keys = k_all[pl.ds(start, window), :]
        values = v_all[pl.ds(start, window), :]
        total = jnp.zeros((tile, width), F32)
        service = pieces(i + 3)
        for h in range(heads):
            masked = jnp.where(lanes == h, queries, jnp.zeros_like(queries))
            gates = (origin[:, h : h + 1] - aux_all[h : h + 1, pl.ds(start, window)]) * LOG2E
            scores = dot_nt(masked, keys) * scale + gates + bias[...]
            peak = jnp.max(scores, axis=-1, keepdims=True)
            weights = jnp.exp2(scores - peak)
            norm = jnp.sum(weights, axis=-1, keepdims=True)
            mixed = dot(weights.astype(BF16), values)
            total = jnp.where(lanes == h, mixed / norm, total)
            if h == heads - 1:
                att[pl.ds(start, tile), own_cols] = total.astype(BF16)
                ats.begin(i)

            @pl.when(i < n_tiles - 1)
            def _():
                service[h]()

        wos.far(i)

        @pl.when(i >= 1)
        def _():
            ats.near(i - 1)

        return carry

    lax.fori_loop(0, n_tiles, attend, 0)
    queue = [piece for r in range(n_tiles + 2, hz + 1) for piece in pieces(r)]

    def serve(count):
        for _ in range(min(count, len(queue))):
            queue.pop(0)()

    n_tile = 256

    def project(i):
        block = pl.ds(i * tile, tile)

        def columns(n, carry):
            cols = pl.ds(pl.multiple_of(n * n_tile, n_tile), n_tile)
            product = dot(att[block, :], wo[:, :, cols].reshape(n_tp * width, n_tile))
            middle[block, cols] = (res[block, cols].astype(F32) + product).astype(BF16)
            return carry

        lax.fori_loop(0, d_model // n_tile, columns, 0)
        wide = middle[block, :].astype(F32)
        factor = lax.rsqrt(jnp.mean(wide * wide, axis=-1, keepdims=True) + EPSILON)
        x_all[block, :] = (wide * factor * gain_ref[...]).astype(BF16)

    ats.far(0)
    wos.far(3)
    ats.near(2)
    serve(2)
    for j in range(4):
        wos.done(j)
    ats.done(0)
    local[6].wait()
    project(0)
    serve(2)
    ats.far(1)
    ats.far(2)
    ats.done(1)
    project(1)
    serve(4)
    ats.done(2)
    project(2)
    serve(len(queue))
    y_turn(hz)

    def rest(r, carry):
        y_arrival(1, -r).wait_recv()
        y_across(-r).wait_recv()
        y_arrival(0, r + 1).wait_recv()
        y_across(r + 1).wait_recv()
        return carry

    lax.fori_loop(0, hz, rest, 0)

    def activate(both, n):
        gate, up = both[:, :128], both[:, 128:]
        hidden[:, pl.ds(pl.multiple_of(n * 128, 128), 128)] = (gate / (1.0 + jnp.exp(-gate)) * up).astype(BF16)

    def expand(n, carry):
        cols = pl.ds(pl.multiple_of(n * 256, 256), 256)
        activate(dot(x_all[...], gu[:, :, cols].reshape(d_model, 256)), n)
        return carry

    lax.fori_loop(0, gu.shape[2] // 256, expand, 0)
    for n in range(extra // 256):
        activate(dot(x_all[...], qd[:, :, n * 256 : (n + 1) * 256].reshape(d_model, 256)), gu.shape[2] // 256 + n)
    group = n_tile // (d_model // n_sp)

    def contract(n, carry):
        cols = pl.ds(pl.multiple_of(n * n_tile, n_tile), n_tile)
        block = qd[pl.ds(n * group, group), :, extra:].reshape(n_tile, ff)
        product = dot_nt(hidden[...], block).astype(BF16)
        part[:, :, :, cols] = product.reshape(nx, 2, rows, n_tile)
        return carry

    lax.fori_loop(0, d_model // n_tile, contract, 0)

    swap = remote(part.at[:, 1 - c], pair, rs_s.at[0], rs_r.at[0], dev_c)
    swap.start()
    swap.wait_recv()

    def on_chip(there):
        return part[there, c].astype(F32) + pair[there].astype(F32)

    opposite, right, left = (x + 2) % nx, (x + 1) % nx, (x + nx - 1) % nx
    total = on_chip(opposite).astype(BF16)
    stage[0] = total[:, :half]
    stage[1] = total[:, half:]
    sends = [swap]

    def send(i, dst, way):
        copy = remote(stage.at[i], dst, rs_s.at[i + 1], rs_r.at[i + 1], dev_x[way])
        copy.start()
        sends.append(copy)
        return copy

    first = send(0, half_in.at[0], 0), send(1, half_in.at[1], 1)
    to_right = on_chip(right)
    to_left = on_chip(left)
    stage[2] = to_right[:, half:].astype(BF16)
    stage[3] = to_left[:, :half].astype(BF16)
    arrivals = [send(2, rs_in.at[0, 1], 0), send(3, rs_in.at[1, 0], 1)]
    own[...] = on_chip(x)
    first[0].wait_recv()
    stage[4] = (to_right[:, :half] + half_in[0].astype(F32)).astype(BF16)
    arrivals.append(send(4, rs_in.at[0, 0], 0))
    first[1].wait_recv()
    stage[5] = (to_left[:, half:] + half_in[1].astype(F32)).astype(BF16)
    arrivals.append(send(5, rs_in.at[1, 1], 1))
    for copy in arrivals:
        copy.wait_recv()
    mine = pl.ds(pl.multiple_of(tp * rows, rows), rows)
    for i in range(2):
        cols = pl.ds(i * half, half)
        down_sum = own[:, cols] + rs_in[0, i].astype(F32) + rs_in[1, i].astype(F32)
        out_ref[:, cols] = (middle[mine, cols].astype(F32) + down_sum).astype(BF16)

    for copy in sends:
        copy.wait_send()
    wos.gone()
    ats.gone()
    for item in ITEMS:
        kv_prev(item).wait_send()
        kv_right(item, last).wait_send()
        kv_left(item, last).wait_send()

        @pl.when((y == 1) | (y == 2))
        def _():
            kv_relay_right(item).wait_send()
            kv_relay_left(item).wait_send()

    for i in range(3):
        d_copy(i).wait_send()

    def gone_z(way, r):
        z_copy(way, r).wait_send()
        for s in range(2):
            q_copy(way, r, s).wait_send()

    def gone_round(r, carry):
        gone_z(0, r)
        gone_z(1, r)
        return carry

    lax.fori_loop(0, hz - 1, gone_round, 0)
    gone_z(1, hz - 1)

    def gone_y(o, carry):
        y_copy(0, o).wait_send()
        y_copy(1, o).wait_send()
        y_across(o).wait_send()
        return carry

    lax.fori_loop(0, nz, gone_y, 0)


def local(n_sp, n_tp, residual, queries, keys, values, gate_cache, doc_ids, out_weight, mix_gain, gate_weight, up_weight, down_weight):
    tok, width = queries.shape
    d_model = out_weight.shape[1]
    rows = tok // n_tp
    wr, ff = gate_weight.shape
    heads = gate_cache.shape[1]
    both = jnp.concatenate(
        [gate_weight.reshape(wr, ff // 128, 1, 128), up_weight.reshape(wr, ff // 128, 1, 128)], axis=2
    ).reshape(wr, 2 * ff)
    early = (2 * ff) // 256 * 256 - 256
    late = jnp.concatenate([both[:, early:], down_weight.T], axis=1)
    aux = jnp.concatenate(
        [gate_cache.T, doc_ids.astype(F32)[None], jnp.zeros((8 - heads - 1, tok), F32)], axis=0
    )
    nz = n_sp // NY
    hz = nz // 2
    tile = 128
    half = d_model // 2
    vmem = pl.BlockSpec(memory_space=pltpu.VMEM)
    anywhere = pl.BlockSpec(memory_space=pl.ANY)
    dma = pltpu.SemaphoreType.DMA
    return pl.pallas_call(
        functools.partial(kernel, n_sp, n_tp),
        out_shape=jax.ShapeDtypeStruct((rows, d_model), BF16),
        in_specs=[vmem, anywhere, anywhere, anywhere, anywhere, anywhere, anywhere, anywhere, vmem],
        out_specs=vmem,
        scratch_shapes=[
            pltpu.VMEM(((REACH + 1) * tok, width), BF16),
            pltpu.VMEM(((REACH + 1) * tok, width), BF16),
            pltpu.VMEM((8, (REACH + 1) * tok), F32),
            pltpu.VMEM((n_sp, wr, early), BF16),
            pltpu.VMEM((n_sp, wr, 3 * ff - early), BF16),
            pltpu.VMEM((n_tp, width, d_model), BF16),
            pltpu.VMEM((tok, d_model), BF16),
            pltpu.VMEM((tile, REACH * tok + tile), F32),
            pltpu.VMEM((tok, 128), F32),
            pltpu.VMEM((tok, n_tp * width), BF16),
            pltpu.VMEM((n_tp // 2, 2, rows, d_model), BF16),
            pltpu.VMEM((n_tp // 2, rows, d_model), BF16),
            pltpu.VMEM((6, rows, half), BF16),
            pltpu.VMEM((rows, d_model), F32),
            pltpu.VMEM((2, rows, half), BF16),
            pltpu.VMEM((2, 2, rows, half), BF16),
            pltpu.VMEM((tok, d_model), BF16),
            pltpu.VMEM((tok, ff), BF16),
            pltpu.VMEM((tok, d_model), BF16),
            dma((7,)),
            dma((3, 5)),
            dma((3, 4)),
            dma((2, hz + 1)),
            dma((2, hz + 1)),
            dma((3, nz)),
            dma((3, nz)),
            dma((3,)),
            dma((3,)),
            dma((2, hz + 1, 2)),
            dma((2, hz + 1, 2)),
            dma((7,)),
            dma((7,)),
            dma((8, 4)),
            dma((8, 4)),
            dma((8, tok // tile)),
            dma((8, tok // tile)),
        ],
        compiler_params=pltpu.CompilerParams(
            collective_id=0, has_side_effects=True, vmem_limit_bytes=60 * 1024 * 1024
        ),
    )(queries, keys, values, aux, both[:, :early], late, out_weight, residual, mix_gain[None])


def solution(mesh):
    n_sp, n_tp = mesh.shape["sp"], mesh.shape["tp"]
    return jax.shard_map(
        functools.partial(local, n_sp, n_tp),
        mesh=mesh,
        in_specs=(
            P("sp", None), P("sp", "tp"), P("sp", "tp"), P("sp", "tp"), P("sp", "tp"), P("sp"),
            P("tp", None), P(), P("sp", "tp"), P("sp", "tp"), P("tp", "sp"),
        ),
        out_specs=P(("sp", "tp"), None),
        check_vma=False,
    )
```

time: 115 us -> 116 us (level)
  other arithmetic: 2.07 us -> 3.47 us
    concatenate x0 -> x1, other arithmetic: none -> 1.4 us  [local(): late = jnp.concatenate([both[:, early:], down_weight.T], axis=1)]
where the time goes in v2:
time: 116 us; the launch traced here: 115 us
  Pallas kernels  107 us (92%)
  local copies, waits for them, and re-layouts  4.16 us (4%)
  other arithmetic  3.47 us (3%)
    pallas_call x1, Pallas kernels, local(): pl.pallas_call(functools.partial(kernel, n_sp, n_tp), out_shape=jax.Shape...  107 us

profile of v2, /device:TPU:1, one launch (start us, length us, event | category | flops | bytes accessed | tf_op | source)
XLA Modules:
  0.0 115.1 jit_solution(15737020075022555101)
XLA Ops:
  0.0 0.1 pad.6.clone
  0.1 0.7 convert_element_type.3
  0.8 1.4 %maximum_maximum_fusion.aux_ref = f32[8,384]{1,0:T(8,128)} fusion(f32[1,384]{1,0:T(1,128)S(1)} %broadcast_in_dim.9, f32[4,384]{1,0:T(4,128)} %bitcast.5, f32[8]{0:T(128)S(1)} %pad.6.clone), kind=kLoop, calls=%fused_computation.2 | loop fusion | flops 6144 | bytes 20000 | tf_op jit(solution)/shard_map/concatenate | solution.py:527
  2.1 0.8 reshape.9
  3.0 0.8 reshape.10
  3.9 0.1 copy.14
  4.0 0.6 slice.8.p_ref
  4.7 1.4 %pad_maximum_fusion.1.d_ref = bf16[32,896]{1,0:T(8,128)(2,1)} fusion(bf16[32,640]{1,0:T(8,128)(2,1)} %bitcast.3, bf16[32,256]{1,0:T(8,128)(2,1)S(1)} %slice.9), kind=kLoop, calls=%fused_computation.1 | loop fusion | flops 114688 | bytes 114688 | tf_op jit(solution)/shard_map/concatenate | solution.py:526
  6.1 107.4 %shard_map.109 = bf16[48,2048]{1,0:T(8,128)(2,1)} custom-call(bf16[384,256]{1,0:T(8,128)(2,1)} %q_ref.1, bf16[384,256]{1,0:T(8,128)(2,1)} %k_ref.1, bf16[384,256]{1,0:T(8,128)(2,1)} %v_ref.1, f32[8,384]{1,0:T(8,128)} %maximum_maximum_fusion.aux_ref, bf16[32,1024]{1,0:T(8,128)(2,1)} %slice.8.p_ref, bf16[32,896]{1,0:T(8,128)(2,1)} %pad_maximum_fusion.1.d_ref, ...), custom_call_target="tpu_custom_call" | custom-call | tf_op jit(solution)/shard_map/pallas_call | solution.py:537
  113.5 1.6 %copy.16 = bf16[48,2048]{1,0:T(8,128)(2,1)} copy(bf16[48,2048]{1,0:T(8,128)(2,1)} %shard_map.109) | data formatting | bytes 393216
  (5 shorter events, 0.1 us)

commit v3 on v2

v3 whole, which is shorter than its diff:
```python
import functools
import math

import jax
import jax.numpy as jnp
from jax import lax
from jax.experimental import pallas as pl
from jax.experimental.pallas import tpu as pltpu
from jax.sharding import PartitionSpec as P

MESH = pl.DeviceIdType.MESH
EPSILON = 1e-06
NEGATIVE = -1e30
REACH = 4
NY = 4
LOG2E = math.log2(math.e)
F32 = jnp.float32
BF16 = jnp.bfloat16


def dot(a, b):
    return lax.dot_general(a, b, (((1,), (0,)), ((), ())), preferred_element_type=F32)


def dot_nt(a, b):
    return lax.dot_general(a, b, (((1,), (1,)), ((), ())), preferred_element_type=F32)


def kernel(
    n_sp, n_tp,
    q_ref, k_ref, v_ref, gates_ref, docs_ref, gate_ref, up_ref, down_ref, wo_ref, res_ref, gain_ref,
    out_ref,
    k_all, v_all, aux_all, gates, down, gu, qd, wo, res, bias, doc_col, att, part, pair,
    stage, own, half_in, rs_in, x_all, hidden, middle,
    loc, kv_s, kv_r, gz_s, gz_r, gy_s, gy_r, dy_s, dy_r, dz_s, dz_r, rs_s, rs_r, wo_s, wo_r, ag_s, ag_r,
):
    nz = n_sp // NY
    nx = n_tp // 2
    hz = nz // 2
    sp, tp = lax.axis_index("sp"), lax.axis_index("tp")
    z, y = sp // NY, sp % NY
    x, c = tp // 2, tp % 2
    tok, width = q_ref.shape
    heads = 4
    rows = tok // n_tp
    d_model = wo.shape[2]
    ff = hidden.shape[1]
    tile = 128
    n_tiles = tok // tile

    def at_sp(dz, dy):
        return ((z + dz + nz) % nz) * NY + (y + dy + NY) % NY

    def at_tp(dx, dc):
        return ((x + dx + nx) % nx) * 2 + (c + dc) % 2

    dev_z = ((at_sp(1, 0), tp), (at_sp(-1, 0), tp))
    dev_y = ((at_sp(0, 1), tp), (at_sp(0, -1), tp), (at_sp(0, 2), tp))
    dev_c = (sp, at_tp(0, 1))
    dev_x = ((sp, at_tp(1, 0)), (sp, at_tp(-1, 0)))

    def remote(src, dst, ssem, rsem, dev):
        return pltpu.make_async_remote_copy(
            src_ref=src, dst_ref=dst, send_sem=ssem, recv_sem=rsem, device_id=dev, device_id_type=MESH
        )

    last = REACH * tok
    extra = qd.shape[2] - ff
    pieces_of = [gu.at[sp, :, pl.ds(j * 128, 128)] for j in range(gu.shape[2] // 128)]
    pieces_of += [qd.at[sp, :, pl.ds(j * 128, 128)] for j in range(extra // 128)]
    local = [
        pltpu.make_async_copy(k_ref, k_all.at[pl.ds(last, tok)], loc.at[0]),
        pltpu.make_async_copy(v_ref, v_all.at[pl.ds(last, tok)], loc.at[1]),
        pltpu.make_async_copy(gates_ref, gates, loc.at[2]),
        pltpu.make_async_copy(down_ref, down, loc.at[3]),
        pltpu.make_async_copy(wo_ref, wo.at[tp], loc.at[4]),
        pltpu.make_async_copy(res_ref, res, loc.at[5]),
    ]
    shards = []
    for j, here in enumerate(pieces_of):
        ref = up_ref if j % 2 else gate_ref
        shards.append(pltpu.make_async_copy(ref.at[:, pl.ds(j // 2 * 128, 128)], here, loc.at[6 + j]))
    for copy in (local[2], local[3], *shards, local[0], local[1], local[4], local[5]):
        copy.start()

    barrier = pltpu.get_barrier_semaphore()
    peers = (*dev_z, *dev_y, dev_c, *dev_x)
    for peer in peers:
        pl.semaphore_signal(barrier, inc=1, device_id=peer, device_id_type=MESH)
    local[2].wait()
    aux_all[:, pl.ds(last, tok)] = jnp.zeros((8, tok), F32)
    aux_all[0:heads, pl.ds(last, tok)] = jnp.transpose(gates[...], (1, 0))
    aux_all[heads : heads + 1, pl.ds(last, tok)] = docs_ref[...].astype(F32)
    local[3].wait()
    turned = jnp.transpose(down[...].astype(F32), (1, 0)).astype(BF16)
    qd[sp, :, extra:] = turned
    pl.semaphore_wait(barrier, len(peers))

    def kv_slot(item, offset):
        if item == 2:
            return aux_all.at[:, pl.ds(pl.multiple_of(offset, 128), tok)]
        return (k_all, v_all)[item].at[pl.ds(pl.multiple_of(offset, 128), tok)]

    def kv_copy(item, kind, src, distance, dev):
        return remote(
            kv_slot(item, src), kv_slot(item, (REACH - distance) * tok),
            kv_s.at[item, kind], kv_r.at[item, distance - 1], dev,
        )

    def kv_prev(item):
        return kv_copy(item, 0, last, 4, dev_z[0])

    def kv_right(item, src):
        return kv_copy(item, 1, src, 1, dev_y[0])

    def kv_left(item, src):
        return kv_copy(item, 2, src, 3, dev_y[1])

    def kv_relay_right(item):
        return kv_copy(item, 3, (REACH - 1) * tok, 2, dev_y[0])

    def kv_relay_left(item):
        return kv_copy(item, 4, (REACH - 3) * tok, 2, dev_y[1])

    ITEMS = (2, 0, 1)

    def kv_own(item):
        if item < 2:
            local[item].wait()
        kv_prev(item).start()

        @pl.when(y < NY - 1)
        def _():
            kv_right(item, last).start()

        @pl.when(y == 0)
        def _():
            kv_left(item, last).start()

    def kv_turn(item):
        kv_prev(item).wait_recv()

        @pl.when(y == NY - 1)
        def _():
            kv_right(item, 0).start()

        @pl.when(y > 0)
        def _():
            kv_left(item, 0).start()

    def kv_relay(item):
        kv_right(item, last).wait_recv()

        @pl.when((y == 1) | (y == 2))
        def _():
            kv_relay_right(item).start()

        kv_left(item, last).wait_recv()

        @pl.when((y == 1) | (y == 2))
        def _():
            kv_relay_left(item).start()

    class Stream:
        def __init__(self, p, near, wide):
            self.p, self.near, self.wide = p, near, wide

        def z_move(self, way, r, step):
            block = self.near.at[at_sp(-r, 0) if way == 0 else at_sp(r, 0)]
            return remote(block, block, gz_s.at[self.p, way, r + step], gz_r.at[self.p, way, r + step], dev_z[way])

        def y_move(self, way, o, dy, lane):
            block, plane = self.near.at[at_sp(o, dy)], (o + nz) % nz
            return remote(block, block, gy_s.at[self.p, lane, plane], gy_r.at[self.p, lane, plane], dev_y[way])

        def y_arrival(self, way, o):
            return self.y_move(way, o, -1 if way == 0 else 1, way)

        def y_across(self, o):
            return self.y_move(0, o, 2, 2)

        def d_move(self, i, dy):
            block = self.wide.at[at_sp(0, dy)]
            return remote(block, block, dy_s.at[self.p, i], dy_r.at[self.p, i], dev_y[i])

        def q_move(self, way, r, s, step):
            plane = (z + (-r if way == 0 else r) + nz) % nz
            block = self.wide.at[pl.ds(plane * NY + s * (NY // 2), NY // 2)]
            return remote(
                block, block, dz_s.at[self.p, way, r + step, s], dz_r.at[self.p, way, r + step, s], dev_z[way]
            )

        def begin_wide(self):
            for i in range(3):
                self.d_move(i, 0).start()

        def begin_near_z(self):
            for way in range(2):
                self.z_move(way, 0, 1).start()

        def begin_near_y(self):
            for way in range(2):
                self.y_move(way, 0, 0, way).start()

        def begin_bundles(self):
            for i in range(3):
                self.d_move(i, (-1, 1, 2)[i]).wait_recv()
            for s in range(2):
                for way in range(2):
                    self.q_move(way, 0, s, 1).start()

        def along_z(self, r):
            fixed = isinstance(r, int)
            for way in range(2):
                count = hz - 1 + way
                if fixed and r > count:
                    continue
                self.z_move(way, r, 0).wait_recv()
                if not fixed or r < count:
                    self.z_move(way, r, 1).start()
                for side in range(2):
                    self.y_move(side, -r if way == 0 else r, 0, side).start()

        def bundles(self, r, s):
            fixed = isinstance(r, int)
            for way in range(2):
                count = hz - 1 + way
                if fixed and r > count:
                    continue
                self.q_move(way, r, s, 0).wait_recv()
                if not fixed or r < count:
                    self.q_move(way, r, s, 1).start()

        def along_y(self, r):
            fixed = isinstance(r, int)
            if not fixed or r < hz:
                self.y_arrival(0, -r).wait_recv()
                self.y_move(0, -r, -1, 2).start()

            def other():
                self.y_arrival(1, r).wait_recv()
                self.y_move(1, r, 1, 2).start()

            if not fixed:
                pl.when(r > 0)(other)
            elif r > 0:
                other()

        def arrive(self, r):
            if r < hz:
                self.y_arrival(1, -r).wait_recv()
                self.y_across(-r).wait_recv()
            if r > 0:
                self.y_arrival(0, r).wait_recv()
                self.y_across(r).wait_recv()

        def pieces(self, k):
            ahead = k + AHEAD
            return [
                functools.partial(self.along_z, ahead),
                functools.partial(self.bundles, k, 0),
                functools.partial(self.along_y, ahead - 1),
                functools.partial(self.bundles, k, 1),
            ]

        def gone(self):
            for i in range(3):
                self.d_move(i, 0).wait_send()

            def ring(way, r):
                self.z_move(way, r, 1).wait_send()
                for s in range(2):
                    self.q_move(way, r, s, 1).wait_send()

            def both(r, carry):
                ring(0, r)
                ring(1, r)
                return carry

            lax.fori_loop(0, hz - 1, both, 0)
            ring(1, hz - 1)

            def side(o, carry):
                for lane in range(3):
                    self.y_move(0, o, 0, lane).wait_send()
                return carry

            lax.fori_loop(0, nz, side, 0)

    AHEAD = 1
    stream = Stream(0, gu, qd)
    queue = []
    for k in range(1, hz + 1):
        steps = stream.pieces(k)
        keep = (k + AHEAD <= hz, True, k + AHEAD - 1 <= hz, True)
        queue += [step for step, wanted in zip(steps, keep) if wanted]

    def serve(count):
        for _ in range(min(count, len(queue))):
            queue.pop(0)()

    class Gather:
        def __init__(self, view, send, recv, count):
            self.view, self.send, self.recv, self.count = view, send, recv, count

        def copy(self, kind, slot, j):
            ref = self.view(slot, j, {2: 0, 3: 1}.get(kind))
            dev = dev_c if kind >= 4 else dev_x[kind % 2]
            return remote(ref, ref, self.send.at[kind, j], self.recv.at[kind, j], dev)

        def begin(self, j):
            for kind in (0, 1, 4):
                self.copy(kind, tp, j).start()

        def near(self, j):
            for way in range(2):
                slot = at_tp(2 * way - 1, 0)
                self.copy(way, slot, j).wait_recv()
                self.copy(2 + way, slot, j).start()
                self.copy(5 + way, slot, j).start()

        def far(self, j):
            slot = at_tp(2, 0)
            self.copy(2, slot, j).wait_recv()
            self.copy(3, slot, j).wait_recv()
            self.copy(7, slot, j).start()

        def done(self, j):
            for kind, dx in ((4, 0), (5, -1), (6, 1), (7, 2)):
                self.copy(kind, at_tp(dx, 1), j).wait_recv()

        def gone(self):
            for kind in range(8):
                for j in range(self.count):
                    self.copy(kind, tp, j).wait_send()

    def wo_view(slot, j, part_of):
        size = width // 4
        if part_of is None:
            return wo.at[slot, pl.ds(j * size, size)]
        return wo.at[slot, pl.ds(j * size + part_of * (size // 2), size // 2)]

    def att_view(slot, j, part_of):
        cols = pl.ds(pl.multiple_of(slot * width, 128), width)
        if part_of is None:
            return att.at[pl.ds(pl.multiple_of(j * tile, tile), tile), cols]
        return att.at[pl.ds(pl.multiple_of(j * tile + part_of * (tile // 2), tile // 2), tile // 2), cols]

    wos = Gather(wo_view, wo_s, wo_r, 4)
    ats = Gather(att_view, ag_s, ag_r, n_tiles)

    for copy in shards:
        copy.wait()
    stream.begin_near_z()
    stream.begin_wide()
    for item in ITEMS:
        kv_own(item)
    stream.begin_near_y()
    local[4].wait()
    for j in range(4):
        wos.begin(j)
    stream.along_z(1)
    stream.begin_bundles()
    kv_turn(2)
    kv_turn(0)
    wos.near(0)
    kv_turn(1)
    stream.along_y(0)
    kv_relay(2)
    kv_relay(0)
    wos.near(1)
    serve(2)
    kv_relay(1)
    serve(2)
    wos.near(2)
    serve(4)
    wos.near(3)
    for item in ITEMS:
        kv_relay_right(item).wait_recv()

    window = REACH * tok + tile
    lanes = lax.broadcasted_iota(jnp.int32, (1, width), 1) // (width // heads)
    scale = (width // heads) ** -0.5 * LOG2E
    own_docs = jnp.transpose(aux_all[:, pl.ds(last, tok)], (1, 0))
    origin = own_docs[0:1, 0:heads]
    doc_col[...] = jnp.broadcast_to(own_docs[:, heads : heads + 1], doc_col.shape)
    own_cols = pl.ds(pl.multiple_of(tp * width, 128), width)

    def attend(i, carry):
        start = pl.multiple_of(i * tile, tile)
        doc_row = aux_all[heads : heads + 1, pl.ds(start, window)]
        doc_here = doc_col[pl.ds(start, tile), 0:1]
        gap = lax.broadcasted_iota(jnp.int32, (tile, window), 1) - lax.broadcasted_iota(jnp.int32, (tile, window), 0)
        bias[...] = jnp.where((doc_row == doc_here) & (gap <= REACH * tok), 0.0, NEGATIVE)
        queries = q_ref[pl.ds(start, tile), :]
        keys = k_all[pl.ds(start, window), :]
        values = v_all[pl.ds(start, window), :]
        total = jnp.zeros((tile, width), F32)
        service = stream.pieces(i + 3)
        for h in range(heads):
            masked = jnp.where(lanes == h, queries, jnp.zeros_like(queries))
            gates = (origin[:, h : h + 1] - aux_all[h : h + 1, pl.ds(start, window)]) * LOG2E
            scores = dot_nt(masked, keys) * scale + gates + bias[...]
            peak = jnp.max(scores, axis=-1, keepdims=True)
            weights = jnp.exp2(scores - peak)
            norm = jnp.sum(weights, axis=-1, keepdims=True)
            mixed = dot(weights.astype(BF16), values)
            total = jnp.where(lanes == h, mixed / norm, total)
            if h == heads - 1:
                att[pl.ds(start, tile), own_cols] = total.astype(BF16)
                ats.begin(i)

            @pl.when(i < n_tiles - 1)
            def _():
                service[h]()

        wos.far(i)

        @pl.when(i >= 1)
        def _():
            ats.near(i - 1)

        return carry

    lax.fori_loop(0, n_tiles, attend, 0)
    del queue[: 4 * (n_tiles - 1)]

    n_tile = 256

    def project(i):
        block = pl.ds(i * tile, tile)

        def columns(n, carry):
            cols = pl.ds(pl.multiple_of(n * n_tile, n_tile), n_tile)
            product = dot(att[block, :], wo[:, :, cols].reshape(n_tp * width, n_tile))
            middle[block, cols] = (res[block, cols].astype(F32) + product).astype(BF16)
            return carry

        lax.fori_loop(0, d_model // n_tile, columns, 0)
        wide = middle[block, :].astype(F32)
        factor = lax.rsqrt(jnp.mean(wide * wide, axis=-1, keepdims=True) + EPSILON)
        x_all[block, :] = (wide * factor * gain_ref[...]).astype(BF16)

    ats.far(0)
    wos.far(3)
    ats.near(2)
    serve(2)
    for j in range(4):
        wos.done(j)
    ats.done(0)
    local[5].wait()
    project(0)
    serve(3)
    ats.far(1)
    ats.far(2)
    ats.done(1)
    project(1)
    serve(3)
    ats.done(2)
    project(2)
    serve(len(queue))
    for r in range(hz + 1):
        stream.arrive(r)

    def activate(both, n):
        gate, up = both[:, :128], both[:, 128:]
        hidden[:, pl.ds(pl.multiple_of(n * 128, 128), 128)] = (gate / (1.0 + jnp.exp(-gate)) * up).astype(BF16)

    early = gu.shape[2] // 256

    def expand(n, carry):
        cols = pl.ds(pl.multiple_of(n * 256, 256), 256)
        activate(dot(x_all[...], gu[:, :, cols].reshape(d_model, 256)), n)
        return carry

    lax.fori_loop(0, early, expand, 0)
    mixed = jnp.concatenate(
        [gu[:, :, early * 256 :].reshape(d_model, 128), qd[:, :, :extra].reshape(d_model, 128)], axis=1
    )
    activate(dot(x_all[...], mixed), early)

    order = [0]
    for r in range(1, hz):
        order += [r, -r]
    order.append(hz)
    groups = [order[i : i + 4] for i in range(0, nz, 4)]
    span = d_model // nz
    sends = []
    half = 2 * span
    opposite, right, left = (x + 2) % nx, (x + 1) % nx, (x + nx - 1) % nx

    def plane_of(o):
        return (z + o + nz) % nz

    def on_chip(g, there):
        return part[g, there, c].astype(F32) + pair[g, there].astype(F32)

    def swap_of(g):
        return remote(part.at[g, :, 1 - c], pair.at[g], rs_s.at[g, 0], rs_r.at[g, 0], dev_c)

    def send_of(g, i):
        dst = (
            half_in.at[g, 0], half_in.at[g, 1], rs_in.at[g, 0, 1], rs_in.at[g, 1, 0], rs_in.at[g, 0, 0], rs_in.at[g, 1, 1]
        )[i]
        return remote(stage.at[g, i], dst, rs_s.at[g, i + 1], rs_r.at[g, i + 1], dev_x[i % 2])

    def contract(g):
        for i in range(2):
            planes = [pl.ds(plane_of(o) * NY, NY) for o in groups[g][2 * i : 2 * i + 2]]
            block = jnp.concatenate([qd[p, :, extra:].reshape(span, ff) for p in planes], axis=0)
            part[g, :, :, :, i * half : (i + 1) * half] = dot_nt(hidden[...], block).astype(BF16).reshape(nx, 2, rows, half)
        swap_of(g).start()

    def outward(g):
        swap_of(g).wait_recv()
        total = on_chip(g, opposite).astype(BF16)
        stage[g, 0] = total[:, :half]
        stage[g, 1] = total[:, half:]
        send_of(g, 0).start()
        send_of(g, 1).start()
        stage[g, 2] = on_chip(g, right)[:, half:].astype(BF16)
        stage[g, 3] = on_chip(g, left)[:, :half].astype(BF16)
        send_of(g, 2).start()
        send_of(g, 3).start()

    def onward(g):
        send_of(g, 0).wait_recv()
        stage[g, 4] = (on_chip(g, right)[:, :half] + half_in[g, 0].astype(F32)).astype(BF16)
        send_of(g, 4).start()
        send_of(g, 1).wait_recv()
        stage[g, 5] = (on_chip(g, left)[:, half:] + half_in[g, 1].astype(F32)).astype(BF16)
        send_of(g, 5).start()

    mine = pl.ds(pl.multiple_of(tp * rows, rows), rows)

    def finish(g):
        own[...] = on_chip(g, x)
        for i in range(2, 6):
            send_of(g, i).wait_recv()
        for j, o in enumerate(groups[g]):
            i, at = j // 2, (j % 2) * span
            cols = pl.ds(pl.multiple_of(plane_of(o) * span, span), span)
            down_sum = (
                own[:, j * span : (j + 1) * span]
                + rs_in[g, 0, i, :, at : at + span].astype(F32)
                + rs_in[g, 1, i, :, at : at + span].astype(F32)
            )
            out_ref[:, cols] = (middle[mine, cols].astype(F32) + down_sum).astype(BF16)

    steps = (contract, outward, onward, finish)
    for t in range(len(groups) + len(steps) - 1):
        for k, step in enumerate(steps):
            if 0 <= t - k < len(groups):
                step(t - k)

    for g in range(len(groups)):
        swap_of(g).wait_send()
        for i in range(6):
            send_of(g, i).wait_send()
    wos.gone()
    ats.gone()
    for item in ITEMS:
        kv_prev(item).wait_send()
        kv_right(item, last).wait_send()
        kv_left(item, last).wait_send()

        @pl.when((y == 1) | (y == 2))
        def _():
            kv_relay_right(item).wait_send()
            kv_relay_left(item).wait_send()

    stream.gone()


def local(n_sp, n_tp, residual, queries, keys, values, gate_cache, doc_ids, out_weight, mix_gain, gate_weight, up_weight, down_weight):
    tok, width = queries.shape
    d_model = out_weight.shape[1]
    rows = tok // n_tp
    wr, ff = gate_weight.shape
    heads = gate_cache.shape[1]
    nz = n_sp // NY
    hz = nz // 2
    tile = 128
    early = 9 * 128
    span = d_model // nz
    n_groups = nz // 4
    vmem = pl.BlockSpec(memory_space=pltpu.VMEM)
    anywhere = pl.BlockSpec(memory_space=pl.ANY)
    dma = pltpu.SemaphoreType.DMA
    return pl.pallas_call(
        functools.partial(kernel, n_sp, n_tp),
        out_shape=jax.ShapeDtypeStruct((rows, d_model), BF16),
        in_specs=[vmem, *[anywhere] * 3, vmem, *[anywhere] * 5, vmem],
        out_specs=vmem,
        scratch_shapes=[
            pltpu.VMEM(((REACH + 1) * tok, width), BF16),
            pltpu.VMEM(((REACH + 1) * tok, width), BF16),
            pltpu.VMEM((8, (REACH + 1) * tok), F32),
            pltpu.VMEM((tok, heads), F32),
            pltpu.VMEM((ff, wr), BF16),
            pltpu.VMEM((n_sp, wr, early), BF16),
            pltpu.VMEM((n_sp, wr, 3 * ff - early), BF16),
            pltpu.VMEM((n_tp, width, d_model), BF16),
            pltpu.VMEM((tok, d_model), BF16),
            pltpu.VMEM((tile, REACH * tok + tile), F32),
            pltpu.VMEM((tok, 128), F32),
            pltpu.VMEM((tok, n_tp * width), BF16),
            pltpu.VMEM((n_groups, n_tp // 2, 2, rows, 4 * span), BF16),
            pltpu.VMEM((n_groups, n_tp // 2, rows, 4 * span), BF16),
            pltpu.VMEM((n_groups, 6, rows, 2 * span), BF16),
            pltpu.VMEM((rows, 4 * span), F32),
            pltpu.VMEM((n_groups, 2, rows, 2 * span), BF16),
            pltpu.VMEM((n_groups, 2, 2, rows, 2 * span), BF16),
            pltpu.VMEM((tok, d_model), BF16),
            pltpu.VMEM((tok, ff), BF16),
            pltpu.VMEM((tok, d_model), BF16),
            dma((6 + ff // 64,)),
            dma((3, 5)),
            dma((3, 4)),
            dma((1, 2, hz + 1)),
            dma((1, 2, hz + 1)),
            dma((1, 3, nz)),
            dma((1, 3, nz)),
            dma((1, 3)),
            dma((1, 3)),
            dma((1, 2, hz + 1, 2)),
            dma((1, 2, hz + 1, 2)),
            dma((n_groups, 7)),
            dma((n_groups, 7)),
            dma((8, 4)),
            dma((8, 4)),
            dma((8, tok // tile)),
            dma((8, tok // tile)),
        ],
        compiler_params=pltpu.CompilerParams(
            collective_id=0, has_side_effects=True, vmem_limit_bytes=60 * 1024 * 1024
        ),
    )(
        queries, keys, values, gate_cache, doc_ids[None], gate_weight, up_weight, down_weight, out_weight, residual, mix_gain[None]
    )


def solution(mesh):
    n_sp, n_tp = mesh.shape["sp"], mesh.shape["tp"]
    return jax.shard_map(
        functools.partial(local, n_sp, n_tp),
        mesh=mesh,
        in_specs=(
            P("sp", None), P("sp", "tp"), P("sp", "tp"), P("sp", "tp"), P("sp", "tp"), P("sp"),
            P("tp", None), P(), P("sp", "tp"), P("sp", "tp"), P("tp", "sp"),
        ),
        out_specs=P(("sp", "tp"), None),
        check_vma=False,
    )
```

time: 116 us -> 112 us (0.966)
  other arithmetic: 3.47 us -> 0 us
  Pallas kernels: 107 us -> 105 us
  local copies, waits for them, and re-layouts: 4.16 us -> 5.94 us
    unnamed x1 -> x3, local copies, waits for them, and re-layouts: 1.62 us -> 4.7 us
    concatenate x3 -> x0, other arithmetic: 2.78 us -> none  [the longest x1 1.4 us: local(): late = jnp.concatenate([both[:, early:], down_weight.T], axis=1)]
    pallas_call x1, Pallas kernels: 107 us -> 105 us  [local(): pl.pallas_call(functools.partial(kernel, n_sp, n_tp), out_shape=jax.Shape...]
    reshape x3 -> x0, local copies, waits for them, and re-layouts: 1.73 us -> none  [the longest x1 0.85 us: local(): up_weight.reshape(wr, ff // 128, 1, 128)]
    broadcast_in_dim x2 -> x1, local copies, waits for them, and re-layouts: 0.01 us -> 1.24 us  [local(): doc_ids[None]]
where the time goes in v3:
time: 112 us; the launch traced here: 111 us
  Pallas kernels  105 us (94%)
  local copies, waits for them, and re-layouts  5.94 us (5%)
    pallas_call x1, Pallas kernels, local(): pl.pallas_call(functools.partial(kernel, n_sp, n_tp), out_shape=jax.Shape...  105 us
    unnamed x3, local copies, waits for them, and re-layouts  4.7 us

profile of v3, /device:TPU:1, one launch (start us, length us, event | category | flops | bytes accessed | tf_op | source)
XLA Modules:
  0.0 111.4 jit_solution(3123617705741669767)
XLA Ops:
  0.0 1.2 %broadcast_in_dim.6.docs_ref = s32[1,384]{1,0:T(1,128)} reshape(s32[384]{0:T(512)} %param.16) | data formatting | bytes 3072 | tf_op jit(solution)/shard_map/broadcast_in_dim | solution.py:639
  1.2 1.6 %copy.13.down_ref = bf16[640,32]{1,0:T(8,128)(2,1)} copy(bf16[640,32]{0,1:T(8,128)(2,1)} %param.21) | data formatting | bytes 81920 | tf_op args[10]
  2.8 1.5 %copy.12.gates_ref = f32[384,4]{1,0:T(8,128)} copy(f32[384,4]{0,1:T(4,128)} %param.15) | data formatting | bytes 12288 | tf_op args[4]
  4.3 105.5 %shard_map.109 = bf16[48,2048]{1,0:T(8,128)(2,1)} custom-call(bf16[384,256]{1,0:T(8,128)(2,1)} %q_ref.1, bf16[384,256]{1,0:T(8,128)(2,1)} %k_ref.1, bf16[384,256]{1,0:T(8,128)(2,1)} %v_ref.1, f32[384,4]{1,0:T(8,128)} %copy.12.gates_ref, s32[1,384]{1,0:T(1,128)} %broadcast_in_dim.6.docs_ref, bf16[32,640]{1,0:T(8,128)(2,1)} %gate_ref.1, ...), custom_call_target="tpu_custom_call" | custom-call | tf_op jit(solution)/shard_map/pallas_call | solution.py:590
  109.8 1.6 %copy.15 = bf16[48,2048]{1,0:T(8,128)(2,1)} copy(bf16[48,2048]{1,0:T(8,128)(2,1)} %shard_map.109) | data formatting | bytes 393216

commit v4 on v3

--- a/solution.py
+++ b/solution.py
@@ -209,42 +209,28 @@
                 for way in range(2):
                     self.q_move(way, 0, s, 1).start()
 
-        def along_z(self, r):
-            fixed = isinstance(r, int)
-            for way in range(2):
-                count = hz - 1 + way
-                if fixed and r > count:
-                    continue
+        def ways(self, k):
+            return [(way, k + way) for way in range(2) if not (isinstance(k, int) and k == 0 and way == 0)]
+
+        def along_z(self, k):
+            for way, r in self.ways(k):
                 self.z_move(way, r, 0).wait_recv()
-                if not fixed or r < count:
+                if not isinstance(k, int) or k < hz - 1:
                     self.z_move(way, r, 1).start()
                 for side in range(2):
                     self.y_move(side, -r if way == 0 else r, 0, side).start()
 
-        def bundles(self, r, s):
-            fixed = isinstance(r, int)
-            for way in range(2):
-                count = hz - 1 + way
-                if fixed and r > count:
-                    continue
+        def bundles(self, k, s):
+            for way, r in self.ways(k):
                 self.q_move(way, r, s, 0).wait_recv()
-                if not fixed or r < count:
+                if not isinstance(k, int) or k < hz - 1:
                     self.q_move(way, r, s, 1).start()
 
-        def along_y(self, r):
-            fixed = isinstance(r, int)
-            if not fixed or r < hz:
-                self.y_arrival(0, -r).wait_recv()
-                self.y_move(0, -r, -1, 2).start()
-
-            def other():
-                self.y_arrival(1, r).wait_recv()
-                self.y_move(1, r, 1, 2).start()
-
-            if not fixed:
-                pl.when(r > 0)(other)
-            elif r > 0:
-                other()
+        def along_y(self, k):
+            self.y_arrival(0, -k).wait_recv()
+            self.y_move(0, -k, -1, 2).start()
+            self.y_arrival(1, k + 1).wait_recv()
+            self.y_move(1, k + 1, 1, 2).start()
 
         def arrive(self, r):
             if r < hz:
@@ -255,11 +241,10 @@
                 self.y_across(r).wait_recv()
 
         def pieces(self, k):
-            ahead = k + AHEAD
             return [
-                functools.partial(self.along_z, ahead),
+                functools.partial(self.along_z, k + 1),
                 functools.partial(self.bundles, k, 0),
-                functools.partial(self.along_y, ahead - 1),
+                functools.partial(self.along_y, k),
                 functools.partial(self.bundles, k, 1),
             ]
 
@@ -287,13 +272,11 @@
 
             lax.fori_loop(0, nz, side, 0)
 
-    AHEAD = 1
     stream = Stream(0, gu, qd)
     queue = []
-    for k in range(1, hz + 1):
+    for k in range(1, hz):
         steps = stream.pieces(k)
-        keep = (k + AHEAD <= hz, True, k + AHEAD - 1 <= hz, True)
-        queue += [step for step, wanted in zip(steps, keep) if wanted]
+        queue += steps if k + 1 < hz else steps[1:]
 
     def serve(count):
         for _ in range(min(count, len(queue))):
@@ -359,12 +342,15 @@
     local[4].wait()
     for j in range(4):
         wos.begin(j)
-    stream.along_z(1)
+    stream.along_z(0)
     stream.begin_bundles()
     kv_turn(2)
     kv_turn(0)
     wos.near(0)
+    stream.bundles(0, 0)
     kv_turn(1)
+    stream.along_z(1)
+    stream.bundles(0, 1)
     stream.along_y(0)
     kv_relay(2)
     kv_relay(0)
@@ -410,9 +396,7 @@
                 att[pl.ds(start, tile), own_cols] = total.astype(BF16)
                 ats.begin(i)
 
-            @pl.when(i < n_tiles - 1)
-            def _():
-                service[h]()
+            service[h]()
 
         wos.far(i)
 
@@ -423,7 +407,7 @@
         return carry
 
     lax.fori_loop(0, n_tiles, attend, 0)
-    del queue[: 4 * (n_tiles - 1)]
+    del queue[: 4 * n_tiles]
 
     n_tile = 256
 
@@ -436,7 +420,10 @@
             middle[block, cols] = (res[block, cols].astype(F32) + product).astype(BF16)
             return carry
 
-        lax.fori_loop(0, d_model // n_tile, columns, 0)
+        cuts = d_model // n_tile // 2
+        lax.fori_loop(0, cuts, columns, 0)
+        serve(1)
+        lax.fori_loop(cuts, 2 * cuts, columns, 0)
         wide = middle[block, :].astype(F32)
         factor = lax.rsqrt(jnp.mean(wide * wide, axis=-1, keepdims=True) + EPSILON)
         x_all[block, :] = (wide * factor * gain_ref[...]).astype(BF16)
@@ -444,18 +431,18 @@
     ats.far(0)
     wos.far(3)
     ats.near(2)
-    serve(2)
+    serve(3)
     for j in range(4):
         wos.done(j)
     ats.done(0)
     local[5].wait()
     project(0)
-    serve(3)
+    serve(1)
     ats.far(1)
     ats.far(2)
     ats.done(1)
     project(1)
-    serve(3)
+    serve(1)
     ats.done(2)
     project(2)
     serve(len(queue))

time: 112 us -> 111 us (level); the launches traced: 111 us -> 109 us
  Pallas kernels: 105 us -> 103 us
    pallas_call x1, Pallas kernels: 105 us -> 103 us  [local(): pl.pallas_call(functools.partial(kernel, n_sp, n_tp), out_shape=jax.Shape...]
where the time goes in v4:
time: 111 us; the launch traced here: 109 us
  Pallas kernels  103 us (93%)
  local copies, waits for them, and re-layouts  5.94 us (5%)
    pallas_call x1, Pallas kernels, local(): pl.pallas_call(functools.partial(kernel, n_sp, n_tp), out_shape=jax.Shape...  103 us
    unnamed x3, local copies, waits for them, and re-layouts  4.7 us

profile of v4, /device:TPU:1, one launch (start us, length us, event | category | flops | bytes accessed | tf_op | source)
XLA Modules:
  0.0 108.9 jit_solution(10908485696860927541)
XLA Ops:
  0.0 1.2 %broadcast_in_dim.6.docs_ref = s32[1,384]{1,0:T(1,128)} reshape(s32[384]{0:T(512)} %param.16) | data formatting | bytes 3072 | tf_op jit(solution)/shard_map/broadcast_in_dim | solution.py:626
  1.2 1.6 %copy.13.down_ref = bf16[640,32]{1,0:T(8,128)(2,1)} copy(bf16[640,32]{0,1:T(8,128)(2,1)} %param.21) | data formatting | bytes 81920 | tf_op args[10]
  2.8 1.5 %copy.12.gates_ref = f32[384,4]{1,0:T(8,128)} copy(f32[384,4]{0,1:T(4,128)} %param.15) | data formatting | bytes 12288 | tf_op args[4]
  4.3 102.9 %shard_map.109 = bf16[48,2048]{1,0:T(8,128)(2,1)} custom-call(bf16[384,256]{1,0:T(8,128)(2,1)} %q_ref.1, bf16[384,256]{1,0:T(8,128)(2,1)} %k_ref.1, bf16[384,256]{1,0:T(8,128)(2,1)} %v_ref.1, f32[384,4]{1,0:T(8,128)} %copy.12.gates_ref, s32[1,384]{1,0:T(1,128)} %broadcast_in_dim.6.docs_ref, bf16[32,640]{1,0:T(8,128)(2,1)} %gate_ref.1, ...), custom_call_target="tpu_custom_call" | custom-call | tf_op jit(solution)/shard_map/pallas_call | solution.py:577
  107.3 1.6 %copy.15 = bf16[48,2048]{1,0:T(8,128)(2,1)} copy(bf16[48,2048]{1,0:T(8,128)(2,1)} %shard_map.109) | data formatting | bytes 393216
